TPU v7x, 32 devices: a whole 2x2x4 slice. The times are simulated.
32 devices in a mesh: ep: 8 (over z, core), tp: 4 (over y, x).
Axes of the slice: x: 2, y: 2, z: 4, core: 2. Of those that a mesh axis runs over, the one named last changes fastest.
Arguments:
- tokens: bfloat16 [256, 2048], P('ep'), may hold values from -6 to 6
- recurrent_head_state: float32 [256, 16, 4096], P('ep', 'tp'), may hold values from -4 to 4
- first_norm_gain: float32 [2048], replicated, may hold values from 0.1 to 1.9
- receptance_matrix: bfloat16 [2048, 1024], P(None, 'tp'), may hold values from -0.125 to 0.125
- key_matrix: bfloat16 [2048, 1024], P(None, 'tp'), may hold values from -0.125 to 0.125
- value_matrix: bfloat16 [2048, 1024], P(None, 'tp'), may hold values from -0.125 to 0.125
- decay_matrix: bfloat16 [2048, 1024], P(None, 'tp'), may hold values from -0.125 to 0.125
- decay_offset: float32 [1024], P('tp'), may hold values from -3 to 0.5
- correction_offset: float32 [1024], P('tp'), may hold values from -2 to 2
- correction_key_factor: float32 [1024], P('tp'), may hold values from -1 to 1
- own_term_weight: float32 [1024], P('tp'), may hold values from -0.9 to 0.9
- head_norm_gain: float32 [1024], P('tp'), may hold values from 0.1 to 1.9
- output_matrix: bfloat16 [1024, 2048], P('tp'), may hold values from -0.1875 to 0.1875
- second_norm_gain: float32 [2048], replicated, may hold values from 0.1 to 1.9
- routing: int32 [256, 2], replicated, may hold values from 0 to 7, all different within a row; in each aligned block of 32 rows (0 to 31, 32 to 63, ...) at most 16 rows name the same one
- routing_weight: float32 [256, 2], P('ep'), may hold values from 0.1 to 1
- expert_gate_weight: bfloat16 [8, 2048, 4096], P('ep', None, 'tp'), may hold values from -0.125 to 0.125
- expert_up_weight: bfloat16 [8, 2048, 4096], P('ep', None, 'tp'), may hold values from -0.125 to 0.125
- expert_down_weight: bfloat16 [8, 4096, 2048], P('ep', 'tp'), may hold values from -0.125 to 0.125
- dense_gate_weight: bfloat16 [2048, 2816], P(None, 'ep'), may hold values from -0.125 to 0.125
- dense_up_weight: bfloat16 [2048, 2816], P(None, 'ep'), may hold values from -0.125 to 0.125
- dense_down_weight: bfloat16 [2816, 2048], P('ep'), may hold values from -0.109375 to 0.109375
- dense_gate_offset: float32 [2048], replicated, may hold values from -3 to 3
Outputs:
- layer_out: bfloat16 [256, 2048], P(('ep', 'tp'))
- next_state: float32 [256, 16, 4096], P('ep', 'tp')
Inputs may be any that keep to these rules, and one draw needn't show every extreme that they name: `routing`: each row names 2 different experts. In each aligned block of 32 rows no expert is named more than 16 times, a bound that some block reaches.
All inputs are finite; a program needn't handle non-finite values.
Results may differ from a plain program's by a relative error of at most 0.017.
Values may be sent and summed in bfloat16 or wider, within the bound.
A program may use at most 64 MiB of HBM per device.

v0:
```python
import functools

import jax
import jax.numpy as jnp
from jax import lax
from jax.experimental import pallas as pl
from jax.experimental.pallas import tpu as pltpu
from jax.sharding import PartitionSpec as P

HEAD_WIDTH = 64
VMEM_BYTES = 67043328


PRECISE = lax.Precision.HIGHEST


def rms_scale(rows, gain):
    floats = rows.astype(jnp.float32)
    return floats * lax.rsqrt(jnp.mean(floats * floats, axis=-1, keepdims=True) + 1e-06) * gain


def route_table(block_routes, experts, capacity):
    flat_routes = block_routes.reshape(-1)
    chosen = (flat_routes[:, None] == jnp.arange(experts, dtype=jnp.int32)[None, :]).astype(
        jnp.int32
    )
    before = jnp.cumsum(chosen, axis=0, dtype=jnp.int32) - chosen
    slot_index = jnp.sum(before * chosen, axis=1)
    slot_match = (slot_index[:, None] == jnp.arange(capacity, dtype=jnp.int32)[None, :]).astype(
        jnp.float32
    )
    dispatch_table = chosen.astype(jnp.float32)[:, :, None] * slot_match[:, None, :]
    return dispatch_table.reshape(block_routes.shape[0], block_routes.shape[1], experts, capacity)


def state_update(
    receptance_rows,
    key_matrix_rows,
    value_matrix_rows,
    decay_logits,
    recurrent_head_state,
    decay_offset,
    correction_offset,
    correction_key_factor,
    own_term_weight,
    head_norm_gain,
    head_width,
):
    seq_count = key_matrix_rows.shape[0]
    decay_factor = jnp.exp(-jnp.exp(decay_offset + decay_logits))
    in_rate = jax.nn.sigmoid(correction_offset + correction_key_factor * key_matrix_rows)
    key_in = key_matrix_rows * in_rate

    def split_heads(block):
        return block.reshape(seq_count, -1, head_width)

    keys_head = split_heads(key_matrix_rows)
    unit_keys = (
        keys_head
        * lax.rsqrt(jnp.mean(keys_head * keys_head, axis=-1, keepdims=True) + 1e-06)
        * head_width ** (-0.5)
    )
    rate_head = split_heads(in_rate)
    head_keys = split_heads(key_in)
    decay_head = split_heads(decay_factor)
    head_values = split_heads(value_matrix_rows)
    head_receptance = split_heads(receptance_rows)
    matrix = recurrent_head_state.reshape(seq_count, -1, head_width, head_width)
    removed = jnp.einsum("bhvk,bhk->bhv", matrix, unit_keys, precision=PRECISE)
    updated = (
        matrix * decay_head[:, :, None, :]
        - removed[..., None] * (unit_keys * rate_head)[:, :, None, :]
        + head_values[..., None] * head_keys[:, :, None, :]
    )
    readout = jnp.einsum("bhvk,bhk->bhv", updated, head_receptance, precision=PRECISE)
    center = jnp.mean(readout, axis=-1, keepdims=True)
    spread = jnp.mean(jnp.square(readout - center), axis=-1, keepdims=True)
    normalized_rows = (
        (readout - center) * lax.rsqrt(spread + 0.00064) * head_norm_gain.reshape(-1, head_width)
    )
    own_term_total = jnp.sum(
        head_receptance * head_keys * own_term_weight.reshape(-1, head_width),
        axis=-1,
        keepdims=True,
    )
    normalized_rows = normalized_rows + own_term_total * head_values
    return (
        normalized_rows.reshape(seq_count, -1).astype(jnp.bfloat16),
        updated.reshape(seq_count, -1, head_width * head_width),
    )


def local(
    tokens,
    recurrent_head_state,
    first_norm_gain,
    receptance_matrix,
    key_matrix,
    value_matrix,
    decay_matrix,
    decay_offset,
    correction_offset,
    correction_key_factor,
    own_term_weight,
    head_norm_gain,
    output_matrix,
    second_norm_gain,
    routing,
    routing_weight,
    expert_gate_weight,
    expert_up_weight,
    expert_down_weight,
    dense_gate_weight,
    dense_up_weight,
    dense_down_weight,
    dense_gate_offset,
):
    seq_count = tokens.shape[0]
    width = tokens.shape[1]
    group_index = lax.axis_index("ep")
    lane_index = lax.axis_index("tp")
    group_count = lax.axis_size("ep")
    lane_count = lax.axis_size("tp")
    normalized_rows = rms_scale(tokens, first_norm_gain).astype(jnp.bfloat16)
    receptance_rows = jnp.dot(
        normalized_rows, receptance_matrix, preferred_element_type=jnp.float32
    )
    key_matrix_rows = jnp.dot(normalized_rows, key_matrix, preferred_element_type=jnp.float32)
    value_matrix_rows = jnp.dot(normalized_rows, value_matrix, preferred_element_type=jnp.float32)
    decay_logits = jnp.dot(normalized_rows, decay_matrix, preferred_element_type=jnp.float32)
    head_outputs, next_state = state_update(
        receptance_rows,
        key_matrix_rows,
        value_matrix_rows,
        decay_logits,
        recurrent_head_state,
        decay_offset,
        correction_offset,
        correction_key_factor,
        own_term_weight,
        head_norm_gain,
        HEAD_WIDTH,
    )
    partial_out = jnp.dot(head_outputs, output_matrix, preferred_element_type=jnp.float32)
    hidden_sum = tokens.astype(jnp.float32) + lax.psum(
        partial_out.astype(jnp.bfloat16), "tp"
    ).astype(jnp.float32)
    ffn_in = rms_scale(hidden_sum, second_norm_gain).astype(jnp.bfloat16)
    local_experts = expert_gate_weight.shape[0]
    top_count = routing.shape[1]
    expert_count = local_experts * group_count
    capacity = 2 * seq_count * top_count // expert_count
    per_lane = seq_count // lane_count
    own_routes = lax.dynamic_slice_in_dim(routing, group_index * seq_count, seq_count, 0)
    own_table = route_table(own_routes, expert_count, capacity)
    send_rows = jnp.einsum(
        "bkec,bd->ecd", own_table.astype(jnp.bfloat16), ffn_in, preferred_element_type=jnp.float32
    ).astype(jnp.bfloat16)
    lane_rows = lax.dynamic_slice_in_dim(ffn_in, lane_index * per_lane, per_lane, 0)
    dense_send = jnp.broadcast_to(lane_rows[None], (group_count, per_lane, width))
    expert_in, dense_in = (
        lax.all_to_all(send_rows, "ep", split_axis=0, concat_axis=0, tiled=True),
        lax.all_to_all(dense_send, "ep", split_axis=0, concat_axis=0, tiled=True),
    )
    rows_in = expert_in.reshape(group_count, local_experts, capacity, width).transpose(1, 0, 2, 3)
    rows_in = rows_in.reshape(local_experts, group_count * capacity, width)
    gate_pre = jnp.einsum(
        "lrd,ldf->lrf", rows_in, expert_gate_weight, preferred_element_type=jnp.float32
    )
    up_pre = jnp.einsum(
        "lrd,ldf->lrf", rows_in, expert_up_weight, preferred_element_type=jnp.float32
    )
    expert_hidden = (jax.nn.silu(gate_pre) * up_pre).astype(jnp.bfloat16)
    expert_part = jnp.einsum(
        "lrf,lfd->lrd", expert_hidden, expert_down_weight, preferred_element_type=jnp.float32
    )
    expert_out = lax.psum_scatter(
        expert_part.astype(jnp.bfloat16), "tp", scatter_dimension=2, tiled=True
    )
    back_send = expert_out.reshape(local_experts, group_count, capacity, -1).transpose(1, 0, 2, 3)
    back_send = back_send.reshape(group_count * local_experts, capacity, -1)
    dense_rows = dense_in.reshape(group_count * per_lane, width)
    dense_hidden = (
        jax.nn.silu(jnp.dot(dense_rows, dense_gate_weight, preferred_element_type=jnp.float32))
        * jnp.dot(dense_rows, dense_up_weight, preferred_element_type=jnp.float32)
    ).astype(jnp.bfloat16)
    dense_part = jnp.dot(
        dense_hidden, dense_down_weight, preferred_element_type=jnp.float32
    ).astype(jnp.bfloat16)
    dense_part = dense_part.reshape(group_count, per_lane, width)
    back_experts, back_dense = (
        lax.all_to_all(back_send, "ep", split_axis=0, concat_axis=0, tiled=True),
        lax.all_to_all(dense_part, "ep", split_axis=0, concat_axis=0, tiled=True),
    )
    dense_sum = jnp.sum(back_dense.astype(jnp.float32), axis=0)
    weighted = jnp.einsum("bkec,bk->ecb", own_table, routing_weight, precision=PRECISE)
    moe_slice = jnp.einsum(
        "ecb,ecd->bd", weighted, back_experts.astype(jnp.float32), precision=PRECISE
    )
    moe_rows = lax.all_to_all(moe_slice, "tp", split_axis=0, concat_axis=1, tiled=True)
    residual_rows = lax.dynamic_slice_in_dim(hidden_sum, lane_index * per_lane, per_lane, 0)
    layer_out = (residual_rows + moe_rows + jax.nn.sigmoid(dense_gate_offset) * dense_sum).astype(
        jnp.bfloat16
    )
    return (layer_out, next_state)


def proj_state_kernel(count, *refs):
    sources, refs = refs[:count], refs[count:]
    state_ref, next_ref, part_ref, base_ref, wext_ref = refs[:5]
    held, (sbuf, nbuf, arg_sem, in_sem, out_sem) = refs[5 : 5 + count], refs[5 + count :]
    (tokens_ref, gain_ref, wr_ref, wk_ref, wv_ref, wd_ref, doff_ref, coff_ref, cfac_ref,
     own_ref, hgain_ref, routes_ref, rweight_ref, wo_ref) = held
    pulls = [
        pltpu.make_async_copy(src, dst, arg_sem.at[i])
        for i, (src, dst) in enumerate(zip(sources, held))
    ]
    for pull in pulls:
        pull.start()
    seqs, width = tokens_ref.shape
    heads = state_ref.shape[1]
    lanes = part_ref.shape[0]
    rows = part_ref.shape[1]
    loads = [
        pltpu.make_async_copy(state_ref.at[:, h, :], sbuf.at[h], in_sem.at[h]) for h in range(heads)
    ]
    for load in loads:
        load.start()
    f32, bf16 = jnp.float32, jnp.bfloat16
    for pull in pulls[:2]:
        pull.wait()
    toks = tokens_ref[...].astype(f32)
    normed = (
        toks * lax.rsqrt(jnp.mean(toks * toks, axis=-1, keepdims=True) + 1e-06) * gain_ref[...]
    ).astype(bf16)
    pulls[2].wait()
    recept = jnp.dot(normed, wr_ref[...], preferred_element_type=f32)
    pulls[3].wait()
    keys = jnp.dot(normed, wk_ref[...], preferred_element_type=f32)
    pulls[4].wait()
    values = jnp.dot(normed, wv_ref[...], preferred_element_type=f32)
    pulls[5].wait()
    logits = jnp.dot(normed, wd_ref[...], preferred_element_type=f32)
    for pull in pulls[6:]:
        pull.wait()
    decay = jnp.exp(-jnp.exp(doff_ref[...] + logits))
    rate = jax.nn.sigmoid(coff_ref[...] + cfac_ref[...] * keys)
    key_in = keys * rate
    own_prod = recept * key_in * own_ref[...]
    hgain = jnp.broadcast_to(hgain_ref[...], keys.shape)
    pair = 2 * HEAD_WIDTH
    lane = lax.broadcasted_iota(jnp.int32, (seqs, pair), 1)
    low = lane < HEAD_WIDTH
    half_r = lax.broadcasted_iota(jnp.int32, (pair, pair), 0) // HEAD_WIDTH
    half_c = lax.broadcasted_iota(jnp.int32, (pair, pair), 1) // HEAD_WIDTH
    ones_block = (half_r == half_c).astype(f32).astype(bf16)

    def group_sum(block):
        high = block.astype(bf16)
        rest = (block - high.astype(f32)).astype(bf16)
        return jnp.dot(high, ones_block, preferred_element_type=f32) + jnp.dot(
            rest, ones_block, preferred_element_type=f32
        )

    def doubled(full, h):
        chunk = full[:, (h // 2) * pair : (h // 2 + 1) * pair]
        turned = pltpu.roll(chunk, HEAD_WIDTH, 1)
        return jnp.where(low, chunk, turned) if h % 2 == 0 else jnp.where(low, turned, chunk)

    chunks = state_ref.shape[2] // pair
    step = 8
    outs, stores = [], []
    for h in range(heads):
        k2, r2, v2 = doubled(keys, h), doubled(recept, h), doubled(values, h)
        d2, kin2, rate2 = doubled(decay, h), doubled(key_in, h), doubled(rate, h)
        unit = (
            k2
            * lax.rsqrt(jnp.mean(k2 * k2, axis=-1, keepdims=True) + 1e-06)
            * HEAD_WIDTH ** (-0.5)
        )
        own_total = 0.5 * jnp.sum(doubled(own_prod, h), axis=-1, keepdims=True)

        def many(block):
            return jnp.concatenate([block] * step, axis=0)

        unit_m, back_m, dec_m = many(unit), many(unit * rate2), many(d2)
        kin_m, rec_m = many(kin2), many(r2)
        loads[h].wait()
        acc = jnp.zeros((seqs, pair), f32)
        for q in range(0, chunks, step):
            picks = [(lane == 2 * j) | (lane == HEAD_WIDTH + 2 * j + 1) for j in range(q, q + step)]
            old = jnp.concatenate(
                [sbuf[h, :, j * pair : (j + 1) * pair] for j in range(q, q + step)], axis=0
            )
            removed = group_sum(old * unit_m)
            spread_v = group_sum(jnp.concatenate([jnp.where(p, v2, 0.0) for p in picks], axis=0))
            new = old * dec_m - removed * back_m + spread_v * kin_m
            for i in range(step):
                nbuf[h, :, (q + i) * pair : (q + i + 1) * pair] = new[i * seqs : (i + 1) * seqs]
            read = group_sum(new * rec_m)
            for i in range(step):
                acc = acc + jnp.where(picks[i], read[i * seqs : (i + 1) * seqs], 0.0)
        store = pltpu.make_async_copy(nbuf.at[h], next_ref.at[:, h, :], out_sem.at[h])
        store.start()
        stores.append(store)
        y = acc + pltpu.roll(acc, HEAD_WIDTH, 1)
        center = y - jnp.mean(y, axis=-1, keepdims=True)
        var = jnp.mean(center * center, axis=-1, keepdims=True)
        outs.append(center * lax.rsqrt(var + 0.00064) * doubled(hgain, h) + own_total * v2)
    merged = jnp.concatenate(
        [jnp.where(low, outs[h], outs[h + 1]) for h in range(0, heads, 2)], axis=1
    ).astype(bf16)
    part = jnp.dot(merged, wo_ref[...], preferred_element_type=f32)
    me_lane = lax.axis_index("tp")
    base = jnp.zeros((rows, width), f32)
    for i in range(lanes):
        mine = part[i * rows : (i + 1) * rows]
        part_ref[i] = mine.astype(bf16)
        base = jnp.where(me_lane == i, mine + toks[i * rows : (i + 1) * rows], base)
    base_ref[...] = base
    start = lax.axis_index("ep") * seqs + me_lane * rows

    def picked_column(ref, k, first):
        spot = lax.broadcasted_iota(jnp.int32, (rows, ref.shape[1]), 1)
        wanted = spot == first + lax.broadcasted_iota(jnp.int32, spot.shape, 0)
        entries = ref[k : k + 1, :].astype(f32)
        return jnp.sum(jnp.where(wanted, entries, 0.0), axis=-1, keepdims=True)

    column = lax.broadcasted_iota(jnp.int32, (rows, 128), 1) % 64
    column = column.astype(f32)
    table = jnp.zeros((rows, 128), f32)
    for k in range(routes_ref.shape[0]):
        expert = picked_column(routes_ref, k, start)
        table = table + jnp.where(
            column == expert, picked_column(rweight_ref, k, me_lane * rows), 0.0
        )
    wext_ref[...] = table
    for store in stores:
        store.wait()


def exchange_kernel(
    groups, lanes,
    part_ref, base_ref, wext_ref, gain_hbm, goff_hbm,
    eg_hbm, eu_hbm, ed_hbm, dg_hbm, du_hbm, dd_hbm,
    out_ref,
    eg, eu, ed, dg, du, dd, gain, goff, hid_rows, p_in, xs, flat, hid, dens, ys, y_in, z_in, v_out, v_in,
    w_sem, s1, r1, sz, rz, st, rt, sc, rc, sa, ra, sb, rb, sv, rv,
):
    f32, bf16 = jnp.float32, jnp.bfloat16
    rows, width = base_ref.shape
    zs = groups // 2
    me_g, me_l = lax.axis_index("ep"), lax.axis_index("tp")
    core, me_z = lax.rem(me_g, 2), me_g // 2
    partner = (me_g + 1 - 2 * core, me_l)

    def lane_peer(d):
        return (me_g, lax.rem(me_l + d + lanes, lanes))

    def z_peer(d):
        return (lax.rem(me_z + d + zs, zs) * 2 + core, me_l)

    def send(src, dst, ssem, rsem, peer):
        copy = pltpu.make_async_remote_copy(
            src_ref=src, dst_ref=dst, send_sem=ssem, recv_sem=rsem, device_id=peer,
            device_id_type=pl.DeviceIdType.MESH,
        )
        copy.start()
        return copy

    pulls = [
        pltpu.make_async_copy(src, dst, w_sem.at[i])
        for i, (src, dst) in enumerate(
            [(gain_hbm, gain), (goff_hbm, goff), (dg_hbm, dg), (du_hbm, du), (dd_hbm, dd), (eg_hbm.at[0], eg), (eu_hbm.at[0], eu),
             (ed_hbm.at[0], ed)]
        )
    ]
    for pull in pulls:
        pull.start()
    barrier = pltpu.get_barrier_semaphore()
    peers = [lane_peer(d) for d in range(1, lanes)] + [z_peer(d) for d in range(1, zs)] + [partner]
    for peer in peers:
        pl.semaphore_signal(barrier, inc=1, device_id=peer, device_id_type=pl.DeviceIdType.MESH)
    pl.semaphore_wait(barrier, len(peers))
    sent = []
    firsts = []
    for d in range(1, lanes):
        target = lax.rem(me_l + lanes - d, lanes)
        firsts.append(
            send(part_ref.at[target], p_in.at[d - 1], s1.at[d - 1], r1.at[d - 1], (me_g, target))
        )
    hidden = base_ref[...]
    for d, copy in enumerate(firsts):
        copy.wait_recv()
        hidden = hidden + p_in[d].astype(f32)
    sent += firsts
    hid_rows[...] = hidden
    for pull in pulls[:2]:
        pull.wait()
    normed = hidden * lax.rsqrt(jnp.mean(hidden * hidden, axis=-1, keepdims=True) + 1e-06)
    xs[0, 0, 0, :, :width] = (normed * gain[...]).astype(bf16)
    table = wext_ref[...]
    high = table.astype(bf16).astype(f32)
    first_half = lax.broadcasted_iota(jnp.int32, table.shape, 1) < 64
    xs[0, 0, 0, :, width:] = jnp.where(first_half, high, table - high).astype(bf16)
    hold_z, hold_t, hold_c = {}, {}, {}
    for d in range(1, zs):
        hold_z[d] = send(xs.at[0, 0, 0], xs.at[0, 0, d], sz.at[d - 1], rz.at[d - 1], z_peer(d))

    def to_partner(d, q):
        i = d * zs + q
        hold_c[d, q] = send(xs.at[0, d, q], xs.at[1, d, q], sc.at[i], rc.at[i], partner)

    def to_lanes(q):
        to_partner(0, q)
        for d in range(1, lanes):
            i = (d - 1) * zs + q
            hold_t[d, q] = send(xs.at[0, 0, q], xs.at[0, d, q], st.at[i], rt.at[i], lane_peer(d))

    to_lanes(0)
    for q in range(1, zs):
        hold_z[q].wait_recv()
        to_lanes(q)
    block = 2 * zs * rows

    def gathered(d):
        return xs[:, d].astype(f32).reshape(block, width + 128)

    for q in range(zs):
        hold_c[0, q].wait_recv()
    mine = gathered(0)
    flat[0:block] = mine.astype(bf16)
    own_rows = mine[:, :width].astype(bf16)
    for pull in pulls[2:5]:
        pull.wait()
    across = (((1,), (1,)), ((), ()))
    gate = lax.dot_general(own_rows, dg[...], across, preferred_element_type=f32)
    up = lax.dot_general(own_rows, du[...], across, preferred_element_type=f32)
    mixed = (jax.nn.silu(gate) * up).astype(bf16)
    dens[...] = jnp.dot(mixed, dd[...], preferred_element_type=f32) * jax.nn.sigmoid(goff[...])
    for q in range(zs):
        for d in range(1, lanes):
            hold_t[d, q].wait_recv()
            to_partner(d, q)
    for d in range(1, lanes):
        for q in range(zs):
            hold_c[d, q].wait_recv()
        flat[d * block : (d + 1) * block] = gathered(d).astype(bf16)
    for pull in pulls[5:]:
        pull.wait()
    tile = 256

    @pl.loop(0, eg.shape[1] // tile, unroll=True)
    def _(n):
        cols = pl.ds(pl.multiple_of(n * tile, tile), tile)
        left = flat[:, :width]
        gated = jnp.dot(left, eg[:, cols], preferred_element_type=f32)
        raised = jnp.dot(left, eu[:, cols], preferred_element_type=f32)
        hid[:, cols] = (jax.nn.silu(gated) * raised).astype(bf16)

    tail = flat[:, width:].astype(f32)
    picked = lax.broadcasted_iota(jnp.int32, tail.shape, 1) % 64 == me_g
    scale = jnp.sum(jnp.where(picked, tail, 0.0), axis=-1, keepdims=True)
    pieces, wide = ys.shape[0], ys.shape[-1]
    to_core, to_lane, to_z = [], [], []

    def pass_on(n):
        to_core[n].wait_recv()
        own = []
        for d in range(1, lanes):
            ys[n, 0, d] = (ys[n, 0, d].astype(f32) + y_in[n, d].astype(f32)).astype(bf16)
            i = n * (lanes - 1) + d - 1
            own.append(
                send(ys.at[n, 0, d], z_in.at[n, d - 1], sb.at[i], rb.at[i], lane_peer(-d))
            )
        to_lane.append(own)

    for n in range(pieces):
        cols = slice(n * wide, (n + 1) * wide)
        made = jnp.dot(hid[...], ed[:, cols], preferred_element_type=f32) * scale
        for d in range(lanes):
            piece = made[d * block : (d + 1) * block]
            if d == 0:
                piece = piece + dens[:, cols]
            ys[n, :, d] = piece.reshape(2, zs, rows, wide).astype(bf16)
        to_core.append(send(ys.at[n, 1], y_in.at[n], sa.at[n], ra.at[n], partner))
        if n > 0:
            pass_on(n - 1)
    pass_on(pieces - 1)
    for n in range(pieces):
        cols = slice(n * wide, (n + 1) * wide)
        total = ys[n, 0, 0].astype(f32) + y_in[n, 0].astype(f32)
        for d in range(1, lanes):
            to_lane[n][d - 1].wait_recv()
            total = total + z_in[n, d - 1].astype(f32)
        v_out[n] = total.astype(bf16)
        own = []
        for d in range(1, zs):
            i = n * (zs - 1) + d - 1
            own.append(
                send(v_out.at[n, d], v_in.at[n, d - 1], sv.at[i], rv.at[i], z_peer(-d))
            )
        to_z.append(own)
        hid_rows[:, cols] = hid_rows[:, cols] + total[0]
    for n in range(pieces):
        cols = slice(n * wide, (n + 1) * wide)
        result = hid_rows[:, cols]
        for d, copy in enumerate(to_z[n]):
            copy.wait_recv()
            result = result + v_in[n, d].astype(f32)
        out_ref[:, cols] = result.astype(bf16)
    sent += list(hold_z.values()) + list(hold_t.values()) + list(hold_c.values())
    sent += to_core
    for own in to_lane + to_z:
        sent += own
    for copy in sent:
        copy.wait_send()


def fused(
    tokens, recurrent_head_state, first_norm_gain, receptance_matrix, key_matrix, value_matrix,
    decay_matrix, decay_offset, correction_offset, correction_key_factor, own_term_weight,
    head_norm_gain, output_matrix, second_norm_gain, routing, routing_weight, expert_gate_weight,
    expert_up_weight, expert_down_weight, dense_gate_weight, dense_up_weight, dense_down_weight,
    dense_gate_offset,
):
    f32, bf16 = jnp.float32, jnp.bfloat16
    seqs, width = tokens.shape
    heads, flat_width = recurrent_head_state.shape[1:]
    groups, lanes = lax.axis_size("ep"), lax.axis_size("tp")
    rows, zs = seqs // lanes, groups // 2
    handed = lanes * rows * width * 2 + rows * width * 4 + rows * 128 * 4
    grant = VMEM_BYTES - handed
    vmem = pl.BlockSpec(memory_space=pltpu.VMEM)
    anywhere = pl.BlockSpec(memory_space=pltpu.HBM)
    dma = pltpu.SemaphoreType.DMA

    def row(vector):
        return vector.reshape(1, -1)

    operands = (
        tokens, row(first_norm_gain), receptance_matrix, key_matrix, value_matrix, decay_matrix,
        row(decay_offset), row(correction_offset), row(correction_key_factor),
        row(own_term_weight), row(head_norm_gain), routing.T, routing_weight.T, output_matrix,
    )
    count = len(operands)
    next_state, part, base, table = pl.pallas_call(
        functools.partial(proj_state_kernel, count),
        out_shape=(
            jax.ShapeDtypeStruct(recurrent_head_state.shape, f32),
            jax.ShapeDtypeStruct((lanes, rows, width), bf16),
            jax.ShapeDtypeStruct((rows, width), f32),
            jax.ShapeDtypeStruct((rows, 128), f32),
        ),
        in_specs=[anywhere] * (count + 1),
        out_specs=(anywhere, vmem, vmem, vmem),
        scratch_shapes=[pltpu.VMEM(operand.shape, operand.dtype) for operand in operands]
        + [
            pltpu.VMEM((heads, seqs, flat_width), f32),
            pltpu.VMEM((heads, seqs, flat_width), f32),
            dma((count,)),
            dma((heads,)),
            dma((heads,)),
        ],
        compiler_params=pltpu.CompilerParams(vmem_limit_bytes=grant),
        name="proj_state",
    )(*operands, recurrent_head_state)
    hidden_units = expert_gate_weight.shape[2]
    pieces = 4
    wide = width // pieces
    total = groups * seqs
    layer_out = pl.pallas_call(
        functools.partial(exchange_kernel, groups, lanes),
        out_shape=jax.ShapeDtypeStruct((rows, width), bf16),
        in_specs=[vmem] * 3 + [anywhere] * 8,
        out_specs=vmem,
        scratch_shapes=[
            pltpu.VMEM(expert_gate_weight.shape[1:], bf16),
            pltpu.VMEM(expert_up_weight.shape[1:], bf16),
            pltpu.VMEM(expert_down_weight.shape[1:], bf16),
            pltpu.VMEM(dense_gate_weight.shape[::-1], bf16),
            pltpu.VMEM(dense_up_weight.shape[::-1], bf16),
            pltpu.VMEM(dense_down_weight.shape, bf16),
            pltpu.VMEM((1, width), f32),
            pltpu.VMEM((1, width), f32),
            pltpu.VMEM((rows, width), f32),
            pltpu.VMEM((lanes - 1, rows, width), bf16),
            pltpu.VMEM((2, lanes, zs, rows, width + 128), bf16),
            pltpu.VMEM((total, width + 128), bf16),
            pltpu.VMEM((total, hidden_units), bf16),
            pltpu.VMEM((2 * zs * rows, width), f32),
            pltpu.VMEM((pieces, 2, lanes, zs, rows, wide), bf16),
            pltpu.VMEM((pieces, lanes, zs, rows, wide), bf16),
            pltpu.VMEM((pieces, lanes - 1, zs, rows, wide), bf16),
            pltpu.VMEM((pieces, zs, rows, wide), bf16),
            pltpu.VMEM((pieces, zs - 1, rows, wide), bf16),
            dma((8,)),
            dma((lanes - 1,)), dma((lanes - 1,)),
            dma((zs - 1,)), dma((zs - 1,)),
            dma(((lanes - 1) * zs,)), dma(((lanes - 1) * zs,)),
            dma((lanes * zs,)), dma((lanes * zs,)),
            dma((pieces,)), dma((pieces,)),
            dma((pieces * (lanes - 1),)), dma((pieces * (lanes - 1),)),
            dma((pieces * (zs - 1),)), dma((pieces * (zs - 1),)),
        ],
        compiler_params=pltpu.CompilerParams(
            collective_id=0, has_side_effects=True, vmem_limit_bytes=grant - rows * width * 2
        ),
        name="exchange",
    )(
        part, base, table, row(second_norm_gain), row(dense_gate_offset), expert_gate_weight,
        expert_up_weight, expert_down_weight, dense_gate_weight.T, dense_up_weight.T,
        dense_down_weight,
    )
    return (layer_out, next_state)


def choose(tokens, recurrent_head_state, *rest):
    groups, lanes = lax.axis_size("ep"), lax.axis_size("tp")
    rows, heads = tokens.shape[0] // lanes, recurrent_head_state.shape[1]
    experts_here = rest[14].shape[0]
    fits = (
        rows % 8 == 0 and heads % 2 == 0 and groups % 2 == 0 and groups > 2 and lanes > 1
        and groups <= 64 and experts_here == 1
    )
    return (fused if fits else local)(tokens, recurrent_head_state, *rest)


def solution(mesh):
    return jax.shard_map(
        choose,
        mesh=mesh,
        in_specs=(
            P("ep", None),
            P("ep", "tp", None),
            P(),
            P(None, "tp"),
            P(None, "tp"),
            P(None, "tp"),
            P(None, "tp"),
            P("tp"),
            P("tp"),
            P("tp"),
            P("tp"),
            P("tp"),
            P("tp", None),
            P(),
            P(),
            P("ep", None),
            P("ep", None, "tp"),
            P("ep", None, "tp"),
            P("ep", "tp", None),
            P(None, "ep"),
            P(None, "ep"),
            P("ep", None),
            P(),
        ),
        out_specs=(P(("ep", "tp"), None), P("ep", "tp", None)),
        check_vma=False,
    )
```

profile of v0, /device:TPU:0, one launch (start us, length us, event | category | flops | bytes accessed | tf_op | source)
XLA Modules:
  0.0 48.8 jit_solution(4703092622779587022)
XLA Ops:
  0.6 9.8 %proj_state.1 = (f32[32,4,4096]{2,1,0:T(4,128)}, bf16[4,8,2048]{2,1,0:T(8,128)(2,1)}, f32[8,2048]{1,0:T(8,128)}, f32[8,128]{1,0:T(8,128)}) custom-call(bf16[32,2048]{1,0:T(8,128)(2,1)} %refs_0_.1, f32[1,2048]{1,0:T(1,128)} %bitcast.14, bf16[2048,256]{1,0:T(8,128)(2,1)} %refs_2_.1, bf16[2048,256]{1,0:T(8,128)(2,1)} %refs_3_.1, bf16[2048,256]{1,0:T(8,128)(2,1)} %refs_4_.1, ...), custom_call_target="tpu_custom_call" | custom-call | tf_op jit(solution)/shard_map/proj_state/pallas_call | solution.py:547
  10.4 37.0 %exchange.1 = bf16[8,2048]{1,0:T(8,128)(2,1)} custom-call(bf16[4,8,2048]{2,1,0:T(8,128)(2,1)} %get-tuple-element.6.part_ref, f32[8,2048]{1,0:T(8,128)} %get-tuple-element.7.base_ref, f32[8,128]{1,0:T(8,128)} %get-tuple-element.8.wext_ref, f32[1,2048]{1,0:T(1,128)} %bitcast.15, f32[1,2048]{1,0:T(1,128)} %bitcast.16, bf16[1,2048,1024]{2,1,0:T(8,128)(2,1)} %eg_hbm.1, ...), custom_call_target="tpu_custom_call" | custom-call | tf_op jit(solution)/shard_map/exchange/pallas_call | solution.py:572
  47.4 1.4 %copy.26 = bf16[8,2048]{1,0:T(8,128)(2,1)} copy(bf16[8,2048]{1,0:T(8,128)(2,1)} %exchange.1) | data formatting | bytes 65536
where the time goes:
time: 49 us; the launch traced here: 48.8 us
  Pallas kernels  46.8 us (96%)
  local copies, waits for them, and re-layouts  1.38 us (3%)
  between operations  0.65 us (1%)
    pallas_call x1, Pallas kernels, fused(): pl.pallas_call(functools.partial(exchange_kernel, groups, lanes), out_sha...  37 us
    pallas_call x1, Pallas kernels, fused(): pl.pallas_call(functools.partial(proj_state_kernel, count), out_shape=(ja...  9.77 us
    unnamed x1, local copies, waits for them, and re-layouts  1.38 us

commit v1 on v0

--- a/solution.py
+++ b/solution.py
@@ -205,150 +205,19 @@
     return (layer_out, next_state)
 
 
-def proj_state_kernel(count, *refs):
+def fused_kernel(count, groups, lanes, *refs):
     sources, refs = refs[:count], refs[count:]
-    state_ref, next_ref, part_ref, base_ref, wext_ref = refs[:5]
-    held, (sbuf, nbuf, arg_sem, in_sem, out_sem) = refs[5 : 5 + count], refs[5 + count :]
-    (tokens_ref, gain_ref, wr_ref, wk_ref, wv_ref, wd_ref, doff_ref, coff_ref, cfac_ref,
-     own_ref, hgain_ref, routes_ref, rweight_ref, wo_ref) = held
-    pulls = [
-        pltpu.make_async_copy(src, dst, arg_sem.at[i])
-        for i, (src, dst) in enumerate(zip(sources, held))
-    ]
-    for pull in pulls:
-        pull.start()
-    seqs, width = tokens_ref.shape
-    heads = state_ref.shape[1]
-    lanes = part_ref.shape[0]
-    rows = part_ref.shape[1]
-    loads = [
-        pltpu.make_async_copy(state_ref.at[:, h, :], sbuf.at[h], in_sem.at[h]) for h in range(heads)
-    ]
-    for load in loads:
-        load.start()
+    state_ref, gain_hbm, goff_hbm, eg_hbm, eu_hbm, ed_hbm, dg_hbm, du_hbm, dd_hbm = refs[:9]
+    nbuf, out_ref = refs[9:11]
+    held, refs = refs[11 : 11 + count], refs[11 + count :]
+    (tokens_ref, gain_ref, doff_ref, coff_ref, cfac_ref, own_ref, hgain_ref, routes_ref,
+     rweight_ref, wk_ref, wd_ref, wr_ref, wv_ref, wo_ref) = held
+    (sbuf, pbuf, gather_ones, spread_ones, spread_in,
+     eg, eu, ed, dg, du, dd, gain, goff, part_ref, hid_rows, p_in, xs, flat, hid, dens,
+     ys, y_in, z_in, v_out, v_in,
+     arg_sem, in_sem,
+     w_sem, s1, r1, sz, rz, st, rt, sc, rc, sa, ra, sb, rb, sv, rv) = refs
     f32, bf16 = jnp.float32, jnp.bfloat16
-    for pull in pulls[:2]:
-        pull.wait()
-    toks = tokens_ref[...].astype(f32)
-    normed = (
-        toks * lax.rsqrt(jnp.mean(toks * toks, axis=-1, keepdims=True) + 1e-06) * gain_ref[...]
-    ).astype(bf16)
-    pulls[2].wait()
-    recept = jnp.dot(normed, wr_ref[...], preferred_element_type=f32)
-    pulls[3].wait()
-    keys = jnp.dot(normed, wk_ref[...], preferred_element_type=f32)
-    pulls[4].wait()
-    values = jnp.dot(normed, wv_ref[...], preferred_element_type=f32)
-    pulls[5].wait()
-    logits = jnp.dot(normed, wd_ref[...], preferred_element_type=f32)
-    for pull in pulls[6:]:
-        pull.wait()
-    decay = jnp.exp(-jnp.exp(doff_ref[...] + logits))
-    rate = jax.nn.sigmoid(coff_ref[...] + cfac_ref[...] * keys)
-    key_in = keys * rate
-    own_prod = recept * key_in * own_ref[...]
-    hgain = jnp.broadcast_to(hgain_ref[...], keys.shape)
-    pair = 2 * HEAD_WIDTH
-    lane = lax.broadcasted_iota(jnp.int32, (seqs, pair), 1)
-    low = lane < HEAD_WIDTH
-    half_r = lax.broadcasted_iota(jnp.int32, (pair, pair), 0) // HEAD_WIDTH
-    half_c = lax.broadcasted_iota(jnp.int32, (pair, pair), 1) // HEAD_WIDTH
-    ones_block = (half_r == half_c).astype(f32).astype(bf16)
-
-    def group_sum(block):
-        high = block.astype(bf16)
-        rest = (block - high.astype(f32)).astype(bf16)
-        return jnp.dot(high, ones_block, preferred_element_type=f32) + jnp.dot(
-            rest, ones_block, preferred_element_type=f32
-        )
-
-    def doubled(full, h):
-        chunk = full[:, (h // 2) * pair : (h // 2 + 1) * pair]
-        turned = pltpu.roll(chunk, HEAD_WIDTH, 1)
-        return jnp.where(low, chunk, turned) if h % 2 == 0 else jnp.where(low, turned, chunk)
-
-    chunks = state_ref.shape[2] // pair
-    step = 8
-    outs, stores = [], []
-    for h in range(heads):
-        k2, r2, v2 = doubled(keys, h), doubled(recept, h), doubled(values, h)
-        d2, kin2, rate2 = doubled(decay, h), doubled(key_in, h), doubled(rate, h)
-        unit = (
-            k2
-            * lax.rsqrt(jnp.mean(k2 * k2, axis=-1, keepdims=True) + 1e-06)
-            * HEAD_WIDTH ** (-0.5)
-        )
-        own_total = 0.5 * jnp.sum(doubled(own_prod, h), axis=-1, keepdims=True)
-
-        def many(block):
-            return jnp.concatenate([block] * step, axis=0)
-
-        unit_m, back_m, dec_m = many(unit), many(unit * rate2), many(d2)
-        kin_m, rec_m = many(kin2), many(r2)
-        loads[h].wait()
-        acc = jnp.zeros((seqs, pair), f32)
-        for q in range(0, chunks, step):
-            picks = [(lane == 2 * j) | (lane == HEAD_WIDTH + 2 * j + 1) for j in range(q, q + step)]
-            old = jnp.concatenate(
-                [sbuf[h, :, j * pair : (j + 1) * pair] for j in range(q, q + step)], axis=0
-            )
-            removed = group_sum(old * unit_m)
-            spread_v = group_sum(jnp.concatenate([jnp.where(p, v2, 0.0) for p in picks], axis=0))
-            new = old * dec_m - removed * back_m + spread_v * kin_m
-            for i in range(step):
-                nbuf[h, :, (q + i) * pair : (q + i + 1) * pair] = new[i * seqs : (i + 1) * seqs]
-            read = group_sum(new * rec_m)
-            for i in range(step):
-                acc = acc + jnp.where(picks[i], read[i * seqs : (i + 1) * seqs], 0.0)
-        store = pltpu.make_async_copy(nbuf.at[h], next_ref.at[:, h, :], out_sem.at[h])
-        store.start()
-        stores.append(store)
-        y = acc + pltpu.roll(acc, HEAD_WIDTH, 1)
-        center = y - jnp.mean(y, axis=-1, keepdims=True)
-        var = jnp.mean(center * center, axis=-1, keepdims=True)
-        outs.append(center * lax.rsqrt(var + 0.00064) * doubled(hgain, h) + own_total * v2)
-    merged = jnp.concatenate(
-        [jnp.where(low, outs[h], outs[h + 1]) for h in range(0, heads, 2)], axis=1
-    ).astype(bf16)
-    part = jnp.dot(merged, wo_ref[...], preferred_element_type=f32)
-    me_lane = lax.axis_index("tp")
-    base = jnp.zeros((rows, width), f32)
-    for i in range(lanes):
-        mine = part[i * rows : (i + 1) * rows]
-        part_ref[i] = mine.astype(bf16)
-        base = jnp.where(me_lane == i, mine + toks[i * rows : (i + 1) * rows], base)
-    base_ref[...] = base
-    start = lax.axis_index("ep") * seqs + me_lane * rows
-
-    def picked_column(ref, k, first):
-        spot = lax.broadcasted_iota(jnp.int32, (rows, ref.shape[1]), 1)
-        wanted = spot == first + lax.broadcasted_iota(jnp.int32, spot.shape, 0)
-        entries = ref[k : k + 1, :].astype(f32)
-        return jnp.sum(jnp.where(wanted, entries, 0.0), axis=-1, keepdims=True)
-
-    column = lax.broadcasted_iota(jnp.int32, (rows, 128), 1) % 64
-    column = column.astype(f32)
-    table = jnp.zeros((rows, 128), f32)
-    for k in range(routes_ref.shape[0]):
-        expert = picked_column(routes_ref, k, start)
-        table = table + jnp.where(
-            column == expert, picked_column(rweight_ref, k, me_lane * rows), 0.0
-        )
-    wext_ref[...] = table
-    for store in stores:
-        store.wait()
-
-
-def exchange_kernel(
-    groups, lanes,
-    part_ref, base_ref, wext_ref, gain_hbm, goff_hbm,
-    eg_hbm, eu_hbm, ed_hbm, dg_hbm, du_hbm, dd_hbm,
-    out_ref,
-    eg, eu, ed, dg, du, dd, gain, goff, hid_rows, p_in, xs, flat, hid, dens, ys, y_in, z_in, v_out, v_in,
-    w_sem, s1, r1, sz, rz, st, rt, sc, rc, sa, ra, sb, rb, sv, rv,
-):
-    f32, bf16 = jnp.float32, jnp.bfloat16
-    rows, width = base_ref.shape
     zs = groups // 2
     me_g, me_l = lax.axis_index("ep"), lax.axis_index("tp")
     core, me_z = lax.rem(me_g, 2), me_g // 2
@@ -368,19 +237,145 @@
         copy.start()
         return copy
 
-    pulls = [
-        pltpu.make_async_copy(src, dst, w_sem.at[i])
-        for i, (src, dst) in enumerate(
-            [(gain_hbm, gain), (goff_hbm, goff), (dg_hbm, dg), (du_hbm, du), (dd_hbm, dd), (eg_hbm.at[0], eg), (eu_hbm.at[0], eu),
-             (ed_hbm.at[0], ed)]
-        )
+    seqs, width = tokens_ref.shape
+    heads = state_ref.shape[1]
+    rows = seqs // lanes
+    args = [
+        pltpu.make_async_copy(src, dst, arg_sem.at[i])
+        for i, (src, dst) in enumerate(zip(sources, held))
     ]
-    for pull in pulls:
-        pull.start()
+    loads = [
+        pltpu.make_async_copy(state_ref.at[:, h, :], sbuf.at[h], in_sem.at[h]) for h in range(heads)
+    ]
+    for arg in args[:-2]:
+        arg.start()
+    for load in loads:
+        load.start()
+    for arg in args[-2:]:
+        arg.start()
     barrier = pltpu.get_barrier_semaphore()
     peers = [lane_peer(d) for d in range(1, lanes)] + [z_peer(d) for d in range(1, zs)] + [partner]
     for peer in peers:
         pl.semaphore_signal(barrier, inc=1, device_id=peer, device_id_type=pl.DeviceIdType.MESH)
+
+    pair = 2 * HEAD_WIDTH
+    flat_width = state_ref.shape[2]
+    tile = 256
+
+    @pl.loop(0, flat_width // tile)
+    def _(n):
+        at = pl.multiple_of(n * tile, tile)
+        r = (lax.broadcasted_iota(jnp.int32, (tile, pair), 0) + at) // HEAD_WIDTH
+        c = lax.broadcasted_iota(jnp.int32, (tile, pair), 1) % HEAD_WIDTH
+        gather_ones[pl.ds(at, tile), :] = (r == c).astype(f32).astype(bf16)
+        r = lax.broadcasted_iota(jnp.int32, (pair, tile), 0) % HEAD_WIDTH
+        c = (lax.broadcasted_iota(jnp.int32, (pair, tile), 1) + at) // HEAD_WIDTH
+        spread_ones[:, pl.ds(at, tile)] = (r == c).astype(f32).astype(bf16)
+
+    half_r = lax.broadcasted_iota(jnp.int32, (pair, pair), 0) // HEAD_WIDTH
+    half_c = lax.broadcasted_iota(jnp.int32, (pair, pair), 1) // HEAD_WIDTH
+    ones_block = (half_r == half_c).astype(f32).astype(bf16)
+
+    def group_sums(*blocks):
+        parts = []
+        for block in blocks:
+            for i in range(0, block.shape[1], pair):
+                piece = block[:, i : i + pair]
+                high = piece.astype(bf16)
+                parts += [high, (piece - high.astype(f32)).astype(bf16)]
+        made = jnp.dot(jnp.concatenate(parts, axis=0), ones_block, preferred_element_type=f32)
+        sums, at = [], 0
+        for block in blocks:
+            cols = []
+            for i in range(0, block.shape[1], pair):
+                cols.append(made[at : at + seqs] + made[at + seqs : at + 2 * seqs])
+                at += 2 * seqs
+            sums.append(jnp.concatenate(cols, axis=1))
+        return sums
+
+    lane = lax.broadcasted_iota(jnp.int32, (seqs, pair), 1)
+    low = lane < HEAD_WIDTH
+
+    def doubled(full, h):
+        chunk = full[:, (h // 2) * pair : (h // 2 + 1) * pair]
+        turned = pltpu.roll(chunk, HEAD_WIDTH, 1)
+        return jnp.where(low, chunk, turned) if h % 2 == 0 else jnp.where(low, turned, chunk)
+
+    for arg in args[:9]:
+        arg.wait()
+    toks = tokens_ref[...].astype(f32)
+    normed = (
+        toks * lax.rsqrt(jnp.mean(toks * toks, axis=-1, keepdims=True) + 1e-06) * gain_ref[...]
+    ).astype(bf16)
+    start = me_g * seqs + me_l * rows
+
+    def picked_column(ref, k, first):
+        spot = lax.broadcasted_iota(jnp.int32, (rows, ref.shape[1]), 1)
+        wanted = spot == first + lax.broadcasted_iota(jnp.int32, spot.shape, 0)
+        entries = ref[k : k + 1, :].astype(f32)
+        return jnp.sum(jnp.where(wanted, entries, 0.0), axis=-1, keepdims=True)
+
+    column = lax.broadcasted_iota(jnp.int32, (rows, 128), 1) % 64
+    column = column.astype(f32)
+    table = jnp.zeros((rows, 128), f32)
+    for k in range(routes_ref.shape[0]):
+        expert = picked_column(routes_ref, k, start)
+        table = table + jnp.where(
+            column == expert, picked_column(rweight_ref, k, me_l * rows), 0.0
+        )
+    high = table.astype(bf16).astype(f32)
+    first_half = lax.broadcasted_iota(jnp.int32, table.shape, 1) < 64
+    xs[0, 0, 0, :, width:] = jnp.where(first_half, high, table - high).astype(bf16)
+
+    args[9].wait()
+    keys = jnp.dot(normed, wk_ref[...], preferred_element_type=f32)
+    (key_squares,) = group_sums(keys * keys)
+    rate = jax.nn.sigmoid(coff_ref[...] + cfac_ref[...] * keys)
+    unit = keys * lax.rsqrt(key_squares * (1.0 / HEAD_WIDTH) + 1e-06) * HEAD_WIDTH ** (-0.5)
+    key_in = keys * rate
+    back = unit * rate
+    args[10].wait()
+    logits = jnp.dot(normed, wd_ref[...], preferred_element_type=f32)
+    decay = jnp.exp(-jnp.exp(doff_ref[...] + logits))
+    args[11].wait()
+    recept = jnp.dot(normed, wr_ref[...], preferred_element_type=f32)
+    faded = decay * recept
+    back_sum, in_sum, own_sum = group_sums(
+        back * recept, key_in * recept, recept * key_in * own_ref[...]
+    )
+    for h in range(heads):
+        u2, f2 = doubled(unit, h), doubled(faded, h)
+        loads[h].wait()
+        for j in range(0, flat_width, pair):
+            old = sbuf[h, :, j : j + pair]
+            pbuf[2 * h * seqs : (2 * h + 1) * seqs, j : j + pair] = (old * u2).astype(bf16)
+            pbuf[(2 * h + 1) * seqs : (2 * h + 2) * seqs, j : j + pair] = (old * f2).astype(bf16)
+    sums = jnp.dot(pbuf[...], gather_ones[...], preferred_element_type=f32)
+    args[12].wait()
+    values = jnp.dot(normed, wv_ref[...], preferred_element_type=f32)
+
+    def merged(first):
+        picks = [sums[(2 * h + first) * seqs : (2 * h + first + 1) * seqs] for h in range(heads)]
+        return jnp.concatenate(
+            [jnp.where(low, picks[h], picks[h + 1]) for h in range(0, heads, 2)], axis=1
+        )
+
+    read = merged(1) - merged(0) * back_sum + values * in_sum
+    (read_sum,) = group_sums(read)
+    center = read - read_sum * (1.0 / HEAD_WIDTH)
+    (square_sum,) = group_sums(center * center)
+    heads_out = (
+        center * lax.rsqrt(square_sum * (1.0 / HEAD_WIDTH) + 0.00064) * hgain_ref[...]
+        + own_sum * values
+    ).astype(bf16)
+    args[13].wait()
+    part = jnp.dot(heads_out, wo_ref[...], preferred_element_type=f32)
+    base = jnp.zeros((rows, width), f32)
+    for i in range(lanes):
+        mine = part[i * rows : (i + 1) * rows]
+        part_ref[i] = mine.astype(bf16)
+        base = jnp.where(me_l == i, mine + toks[i * rows : (i + 1) * rows], base)
+    hid_rows[...] = base
     pl.semaphore_wait(barrier, len(peers))
     sent = []
     firsts = []
@@ -389,7 +384,42 @@
         firsts.append(
             send(part_ref.at[target], p_in.at[d - 1], s1.at[d - 1], r1.at[d - 1], (me_g, target))
         )
-    hidden = base_ref[...]
+    pulls = [
+        pltpu.make_async_copy(src, dst, w_sem.at[i])
+        for i, (src, dst) in enumerate(
+            [(gain_hbm, gain), (goff_hbm, goff), (dg_hbm, dg), (du_hbm, du), (dd_hbm, dd),
+             (eg_hbm.at[0], eg), (eu_hbm.at[0], eu), (ed_hbm.at[0], ed)]
+        )
+    ]
+    for pull in pulls:
+        pull.start()
+
+    def halves(block):
+        high = block.astype(bf16).astype(f32)
+        return jnp.where(low, high, block - high).astype(bf16)
+
+    for h in range(heads):
+        spread_in[2 * h * seqs : (2 * h + 1) * seqs] = halves(
+            sums[2 * h * seqs : (2 * h + 1) * seqs]
+        )
+        spread_in[(2 * h + 1) * seqs : (2 * h + 2) * seqs] = halves(doubled(values, h))
+    fades = [doubled(decay, h) for h in range(heads)]
+    backs = [doubled(back, h) for h in range(heads)]
+    ins = [doubled(key_in, h) for h in range(heads)]
+    for n in range(0, flat_width, tile):
+        wide_rows = jnp.dot(
+            spread_in[...], spread_ones[:, n : n + tile], preferred_element_type=f32
+        )
+        for h in range(heads):
+            gone = wide_rows[2 * h * seqs : (2 * h + 1) * seqs]
+            came = wide_rows[(2 * h + 1) * seqs : (2 * h + 2) * seqs]
+            for i in range(0, tile, pair):
+                nbuf[h, :, n + i : n + i + pair] = (
+                    sbuf[h, :, n + i : n + i + pair] * fades[h]
+                    - gone[:, i : i + pair] * backs[h]
+                    + came[:, i : i + pair] * ins[h]
+                )
+    hidden = hid_rows[...]
     for d, copy in enumerate(firsts):
         copy.wait_recv()
         hidden = hidden + p_in[d].astype(f32)
@@ -399,10 +429,6 @@
         pull.wait()
     normed = hidden * lax.rsqrt(jnp.mean(hidden * hidden, axis=-1, keepdims=True) + 1e-06)
     xs[0, 0, 0, :, :width] = (normed * gain[...]).astype(bf16)
-    table = wext_ref[...]
-    high = table.astype(bf16).astype(f32)
-    first_half = lax.broadcasted_iota(jnp.int32, table.shape, 1) < 64
-    xs[0, 0, 0, :, width:] = jnp.where(first_half, high, table - high).astype(bf16)
     hold_z, hold_t, hold_c = {}, {}, {}
     for d in range(1, zs):
         hold_z[d] = send(xs.at[0, 0, 0], xs.at[0, 0, d], sz.at[d - 1], rz.at[d - 1], z_peer(d))
@@ -448,7 +474,6 @@
         flat[d * block : (d + 1) * block] = gathered(d).astype(bf16)
     for pull in pulls[5:]:
         pull.wait()
-    tile = 256
 
     @pl.loop(0, eg.shape[1] // tile, unroll=True)
     def _(n):
@@ -517,6 +542,18 @@
         copy.wait_send()
 
 
+def hand_over_kernel(rows_ref, state_ref, out_ref, next_ref, row_sem, state_sem):
+    heads = state_ref.shape[0]
+    copies = [pltpu.make_async_copy(rows_ref, out_ref, row_sem)] + [
+        pltpu.make_async_copy(state_ref.at[h], next_ref.at[:, h, :], state_sem.at[h])
+        for h in range(heads)
+    ]
+    for copy in copies:
+        copy.start()
+    for copy in copies:
+        copy.wait()
+
+
 def fused(
     tokens, recurrent_head_state, first_norm_gain, receptance_matrix, key_matrix, value_matrix,
     decay_matrix, decay_offset, correction_offset, correction_key_factor, own_term_weight,
@@ -529,8 +566,7 @@
     heads, flat_width = recurrent_head_state.shape[1:]
     groups, lanes = lax.axis_size("ep"), lax.axis_size("tp")
     rows, zs = seqs // lanes, groups // 2
-    handed = lanes * rows * width * 2 + rows * width * 4 + rows * 128 * 4
-    grant = VMEM_BYTES - handed
+    grant = VMEM_BYTES - rows * width * 2 - heads * seqs * flat_width * 4
     vmem = pl.BlockSpec(memory_space=pltpu.VMEM)
     anywhere = pl.BlockSpec(memory_space=pltpu.HBM)
     dma = pltpu.SemaphoreType.DMA
@@ -539,42 +575,31 @@
         return vector.reshape(1, -1)
 
     operands = (
-        tokens, row(first_norm_gain), receptance_matrix, key_matrix, value_matrix, decay_matrix,
-        row(decay_offset), row(correction_offset), row(correction_key_factor),
-        row(own_term_weight), row(head_norm_gain), routing.T, routing_weight.T, output_matrix,
+        tokens, row(first_norm_gain), row(decay_offset), row(correction_offset),
+        row(correction_key_factor), row(own_term_weight), row(head_norm_gain), routing.T,
+        routing_weight.T, key_matrix, decay_matrix, receptance_matrix, value_matrix, output_matrix,
     )
     count = len(operands)
-    next_state, part, base, table = pl.pallas_call(
-        functools.partial(proj_state_kernel, count),
-        out_shape=(
-            jax.ShapeDtypeStruct(recurrent_head_state.shape, f32),
-            jax.ShapeDtypeStruct((lanes, rows, width), bf16),
-            jax.ShapeDtypeStruct((rows, width), f32),
-            jax.ShapeDtypeStruct((rows, 128), f32),
-        ),
-        in_specs=[anywhere] * (count + 1),
-        out_specs=(anywhere, vmem, vmem, vmem),
-        scratch_shapes=[pltpu.VMEM(operand.shape, operand.dtype) for operand in operands]
-        + [
-            pltpu.VMEM((heads, seqs, flat_width), f32),
-            pltpu.VMEM((heads, seqs, flat_width), f32),
-            dma((count,)),
-            dma((heads,)),
-            dma((heads,)),
-        ],
-        compiler_params=pltpu.CompilerParams(vmem_limit_bytes=grant),
-        name="proj_state",
-    )(*operands, recurrent_head_state)
     hidden_units = expert_gate_weight.shape[2]
     pieces = 4
     wide = width // pieces
     total = groups * seqs
-    layer_out = pl.pallas_call(
-        functools.partial(exchange_kernel, groups, lanes),
-        out_shape=jax.ShapeDtypeStruct((rows, width), bf16),
-        in_specs=[vmem] * 3 + [anywhere] * 8,
-        out_specs=vmem,
-        scratch_shapes=[
+    pair = 2 * HEAD_WIDTH
+    next_state, layer_rows = pl.pallas_call(
+        functools.partial(fused_kernel, count, groups, lanes),
+        out_shape=(
+            jax.ShapeDtypeStruct((heads, seqs, flat_width), f32),
+            jax.ShapeDtypeStruct((rows, width), bf16),
+        ),
+        in_specs=[anywhere] * (count + 9),
+        out_specs=(vmem, vmem),
+        scratch_shapes=[pltpu.VMEM(operand.shape, operand.dtype) for operand in operands]
+        + [
+            pltpu.VMEM((heads, seqs, flat_width), f32),
+            pltpu.VMEM((2 * heads * seqs, flat_width), bf16),
+            pltpu.VMEM((flat_width, pair), bf16),
+            pltpu.VMEM((pair, flat_width), bf16),
+            pltpu.VMEM((2 * heads * seqs, pair), bf16),
             pltpu.VMEM(expert_gate_weight.shape[1:], bf16),
             pltpu.VMEM(expert_up_weight.shape[1:], bf16),
             pltpu.VMEM(expert_down_weight.shape[1:], bf16),
@@ -583,6 +608,7 @@
             pltpu.VMEM(dense_down_weight.shape, bf16),
             pltpu.VMEM((1, width), f32),
             pltpu.VMEM((1, width), f32),
+            pltpu.VMEM((lanes, rows, width), bf16),
             pltpu.VMEM((rows, width), f32),
             pltpu.VMEM((lanes - 1, rows, width), bf16),
             pltpu.VMEM((2, lanes, zs, rows, width + 128), bf16),
@@ -594,6 +620,8 @@
             pltpu.VMEM((pieces, lanes - 1, zs, rows, wide), bf16),
             pltpu.VMEM((pieces, zs, rows, wide), bf16),
             pltpu.VMEM((pieces, zs - 1, rows, wide), bf16),
+            dma((count,)),
+            dma((heads,)),
             dma((8,)),
             dma((lanes - 1,)), dma((lanes - 1,)),
             dma((zs - 1,)), dma((zs - 1,)),
@@ -604,15 +632,25 @@
             dma((pieces * (zs - 1),)), dma((pieces * (zs - 1),)),
         ],
         compiler_params=pltpu.CompilerParams(
-            collective_id=0, has_side_effects=True, vmem_limit_bytes=grant - rows * width * 2
+            collective_id=0, has_side_effects=True, vmem_limit_bytes=grant
         ),
-        name="exchange",
+        name="layer",
     )(
-        part, base, table, row(second_norm_gain), row(dense_gate_offset), expert_gate_weight,
-        expert_up_weight, expert_down_weight, dense_gate_weight.T, dense_up_weight.T,
-        dense_down_weight,
-    )
-    return (layer_out, next_state)
+        *operands, recurrent_head_state, row(second_norm_gain), row(dense_gate_offset),
+        expert_gate_weight, expert_up_weight, expert_down_weight, dense_gate_weight.T,
+        dense_up_weight.T, dense_down_weight,
+    )
+    return pl.pallas_call(
+        hand_over_kernel,
+        out_shape=(
+            jax.ShapeDtypeStruct((rows, width), bf16),
+            jax.ShapeDtypeStruct(recurrent_head_state.shape, f32),
+        ),
+        in_specs=[vmem, vmem],
+        out_specs=(anywhere, anywhere),
+        scratch_shapes=[dma, dma((heads,))],
+        name="hand_over",
+    )(layer_rows, next_state)
 
 
 def choose(tokens, recurrent_head_state, *rest):

time: 49 us -> 44.2 us (0.902)
  Pallas kernels: 46.8 us -> 43.4 us
  local copies, waits for them, and re-layouts: 1.38 us -> 0 us
    pallas_call x2, Pallas kernels: 46.8 us -> 43.4 us  [the longest x1 40.4 us: fused(): pl.pallas_call(functools.partial(fused_kernel, count, groups, lanes), out...]
    unnamed x1 -> x0, local copies, waits for them, and re-layouts: 1.38 us -> none
where the time goes in v1:
time: 44.2 us; the launch traced here: 44.1 us
  Pallas kernels  43.4 us (98%)
  between operations  0.65 us (1%)
    pallas_call x1, Pallas kernels, fused(): pl.pallas_call(functools.partial(fused_kernel, count, groups, lanes), out...  40.4 us
    pallas_call x1, Pallas kernels, fused(): pl.pallas_call(hand_over_kernel, out_shape=(jax.ShapeDtypeStruct((rows, w...  2.98 us

profile of v1, /device:TPU:0, one launch (start us, length us, event | category | flops | bytes accessed | tf_op | source)
XLA Modules:
  0.0 44.1 jit_solution(10882369011894162058)
XLA Ops:
  0.6 40.4 %layer.1 = (f32[4,32,4096]{2,1,0:T(8,128)}, bf16[8,2048]{1,0:T(8,128)(2,1)}) custom-call(bf16[32,2048]{1,0:T(8,128)(2,1)} %refs_0_.1, f32[1,2048]{1,0:T(1,128)} %bitcast.14, f32[1,256]{1,0:T(1,128)} %bitcast.18, f32[1,256]{1,0:T(1,128)} %bitcast.19, f32[1,256]{1,0:T(1,128)} %bitcast.20, f32[1,256]{1,0:T(1,128)} %bitcast.21, f32[1,256]{1,0:T(1,128)} %bitcast.22, ...), custom_call_target="tpu_custom_call" | custom-call | tf_op jit(solution)/shard_map/layer/pallas_call | solution.py:588
  41.1 3.0 %hand_over.1 = (bf16[8,2048]{1,0:T(8,128)(2,1)}, f32[32,4,4096]{2,1,0:T(4,128)}) custom-call(bf16[8,2048]{1,0:T(8,128)(2,1)} %get-tuple-element.4.rows_ref, f32[4,32,4096]{2,1,0:T(8,128)} %get-tuple-element.5.state_ref), custom_call_target="tpu_custom_call" | custom-call | tf_op jit(solution)/shard_map/hand_over/pallas_call | solution.py:643

commit v2 on v1

--- a/solution.py
+++ b/solution.py
@@ -214,17 +214,25 @@
      rweight_ref, wk_ref, wd_ref, wr_ref, wv_ref, wo_ref) = held
     (sbuf, pbuf, gather_ones, spread_ones, spread_in,
      eg, eu, ed, dg, du, dd, gain, goff, part_ref, hid_rows, p_in, xs, flat, hid, dens,
-     ys, y_in, z_in, v_out, v_in,
+     ys, y_in, z_in, v_out, v_in, dg_in, d_out, d_in,
      arg_sem, in_sem,
-     w_sem, s1, r1, sz, rz, st, rt, sc, rc, sa, ra, sb, rb, sv, rv) = refs
+     w_sem, s1, r1, st, rt, sc, rc, sa, ra, sb, rb, sv, rv, sg, rg, sd, rd) = refs
     f32, bf16 = jnp.float32, jnp.bfloat16
     zs = groups // 2
     me_g, me_l = lax.axis_index("ep"), lax.axis_index("tp")
     core, me_z = lax.rem(me_g, 2), me_g // 2
     partner = (me_g + 1 - 2 * core, me_l)
 
+    side_x, side_y = lax.rem(me_l, 2), me_l // 2
+
+    def lane_at(d):
+        flip_x, flip_y = d % 2, d // 2
+        x = side_x + flip_x - 2 * flip_x * side_x
+        y = side_y + flip_y - 2 * flip_y * side_y
+        return 2 * y + x
+
     def lane_peer(d):
-        return (me_g, lax.rem(me_l + d + lanes, lanes))
+        return (me_g, lane_at(d))
 
     def z_peer(d):
         return (lax.rem(me_z + d + zs, zs) * 2 + core, me_l)
@@ -262,15 +270,12 @@
     flat_width = state_ref.shape[2]
     tile = 256
 
-    @pl.loop(0, flat_width // tile)
-    def _(n):
-        at = pl.multiple_of(n * tile, tile)
-        r = (lax.broadcasted_iota(jnp.int32, (tile, pair), 0) + at) // HEAD_WIDTH
-        c = lax.broadcasted_iota(jnp.int32, (tile, pair), 1) % HEAD_WIDTH
-        gather_ones[pl.ds(at, tile), :] = (r == c).astype(f32).astype(bf16)
-        r = lax.broadcasted_iota(jnp.int32, (pair, tile), 0) % HEAD_WIDTH
-        c = (lax.broadcasted_iota(jnp.int32, (pair, tile), 1) + at) // HEAD_WIDTH
-        spread_ones[:, pl.ds(at, tile)] = (r == c).astype(f32).astype(bf16)
+    offset = (
+        lax.broadcasted_iota(jnp.int32, (tile, pair), 0) // HEAD_WIDTH
+        - lax.broadcasted_iota(jnp.int32, (tile, pair), 1) % HEAD_WIDTH
+    )
+    for n in range(0, flat_width, tile):
+        gather_ones[n : n + tile, :] = jnp.where(offset == -(n // HEAD_WIDTH), 1.0, 0.0).astype(bf16)
 
     half_r = lax.broadcasted_iota(jnp.int32, (pair, pair), 0) // HEAD_WIDTH
     half_c = lax.broadcasted_iota(jnp.int32, (pair, pair), 1) // HEAD_WIDTH
@@ -329,30 +334,31 @@
 
     args[9].wait()
     keys = jnp.dot(normed, wk_ref[...], preferred_element_type=f32)
+    args[10].wait()
+    logits = jnp.dot(normed, wd_ref[...], preferred_element_type=f32)
+    args[11].wait()
+    recept = jnp.dot(normed, wr_ref[...], preferred_element_type=f32)
+    for load in loads:
+        load.wait()
+    args[12].wait()
+    values = jnp.dot(normed, wv_ref[...], preferred_element_type=f32)
     (key_squares,) = group_sums(keys * keys)
     rate = jax.nn.sigmoid(coff_ref[...] + cfac_ref[...] * keys)
     unit = keys * lax.rsqrt(key_squares * (1.0 / HEAD_WIDTH) + 1e-06) * HEAD_WIDTH ** (-0.5)
     key_in = keys * rate
     back = unit * rate
-    args[10].wait()
-    logits = jnp.dot(normed, wd_ref[...], preferred_element_type=f32)
     decay = jnp.exp(-jnp.exp(doff_ref[...] + logits))
-    args[11].wait()
-    recept = jnp.dot(normed, wr_ref[...], preferred_element_type=f32)
     faded = decay * recept
     back_sum, in_sum, own_sum = group_sums(
         back * recept, key_in * recept, recept * key_in * own_ref[...]
     )
     for h in range(heads):
         u2, f2 = doubled(unit, h), doubled(faded, h)
-        loads[h].wait()
         for j in range(0, flat_width, pair):
             old = sbuf[h, :, j : j + pair]
             pbuf[2 * h * seqs : (2 * h + 1) * seqs, j : j + pair] = (old * u2).astype(bf16)
             pbuf[(2 * h + 1) * seqs : (2 * h + 2) * seqs, j : j + pair] = (old * f2).astype(bf16)
     sums = jnp.dot(pbuf[...], gather_ones[...], preferred_element_type=f32)
-    args[12].wait()
-    values = jnp.dot(normed, wv_ref[...], preferred_element_type=f32)
 
     def merged(first):
         picks = [sums[(2 * h + first) * seqs : (2 * h + first + 1) * seqs] for h in range(heads)]
@@ -379,10 +385,12 @@
     pl.semaphore_wait(barrier, len(peers))
     sent = []
     firsts = []
-    for d in range(1, lanes):
-        target = lax.rem(me_l + lanes - d, lanes)
+    across = lanes - 1
+    for d in (across, 1, 2):
         firsts.append(
-            send(part_ref.at[target], p_in.at[d - 1], s1.at[d - 1], r1.at[d - 1], (me_g, target))
+            send(
+                part_ref.at[lane_at(d)], p_in.at[d - 1], s1.at[d - 1], r1.at[d - 1], lane_peer(d)
+            )
         )
     pulls = [
         pltpu.make_async_copy(src, dst, w_sem.at[i])
@@ -393,6 +401,13 @@
     ]
     for pull in pulls:
         pull.start()
+
+    offset = (
+        lax.broadcasted_iota(jnp.int32, (pair, tile), 0) % HEAD_WIDTH
+        - lax.broadcasted_iota(jnp.int32, (pair, tile), 1) // HEAD_WIDTH
+    )
+    for n in range(0, flat_width, tile):
+        spread_ones[:, n : n + tile] = jnp.where(offset == n // HEAD_WIDTH, 1.0, 0.0).astype(bf16)
 
     def halves(block):
         high = block.astype(bf16).astype(f32)
@@ -420,33 +435,51 @@
                     + came[:, i : i + pair] * ins[h]
                 )
     hidden = hid_rows[...]
-    for d, copy in enumerate(firsts):
+    for copy in firsts:
         copy.wait_recv()
-        hidden = hidden + p_in[d].astype(f32)
+    for d in range(1, lanes):
+        hidden = hidden + p_in[d - 1].astype(f32)
     sent += firsts
     hid_rows[...] = hidden
     for pull in pulls[:2]:
         pull.wait()
     normed = hidden * lax.rsqrt(jnp.mean(hidden * hidden, axis=-1, keepdims=True) + 1e-06)
     xs[0, 0, 0, :, :width] = (normed * gain[...]).astype(bf16)
-    hold_z, hold_t, hold_c = {}, {}, {}
-    for d in range(1, zs):
-        hold_z[d] = send(xs.at[0, 0, 0], xs.at[0, 0, d], sz.at[d - 1], rz.at[d - 1], z_peer(d))
+    hold = {}
+
+    def pass_block(d, q, to_d, to_q, peer):
+        i = to_d * zs + to_q
+        hold[to_d, to_q] = send(xs.at[0, d, q], xs.at[0, to_d, to_q], st.at[i], rt.at[i], peer)
+
+    hold_c = {}
 
     def to_partner(d, q):
         i = d * zs + q
         hold_c[d, q] = send(xs.at[0, d, q], xs.at[1, d, q], sc.at[i], rc.at[i], partner)
 
-    def to_lanes(q):
+    pass_block(0, 0, across, 0, lane_peer(across))
+    for q in range(1, zs):
+        pass_block(0, 0, 0, q, z_peer(q))
+    for d in (1, 2):
+        pass_block(0, 0, d, 0, lane_peer(d))
+    to_partner(0, 0)
+
+    def spread_row(q):
+        hold[0, q].wait_recv()
+        for d in (1, 2):
+            pass_block(0, q, d, q, lane_peer(d))
         to_partner(0, q)
-        for d in range(1, lanes):
-            i = (d - 1) * zs + q
-            hold_t[d, q] = send(xs.at[0, 0, q], xs.at[0, d, q], st.at[i], rt.at[i], lane_peer(d))
-
-    to_lanes(0)
+
+    spread_row(1)
+    hold[across, 0].wait_recv()
     for q in range(1, zs):
-        hold_z[q].wait_recv()
-        to_lanes(q)
+        pass_block(across, 0, across, q, z_peer(q))
+    for q in range(2, zs):
+        spread_row(q)
+    to_partner(across, 0)
+    for d in (1, 2):
+        hold[d, 0].wait_recv()
+        to_partner(d, 0)
     block = 2 * zs * rows
 
     def gathered(d):
@@ -459,14 +492,14 @@
     own_rows = mine[:, :width].astype(bf16)
     for pull in pulls[2:5]:
         pull.wait()
-    across = (((1,), (1,)), ((), ()))
-    gate = lax.dot_general(own_rows, dg[...], across, preferred_element_type=f32)
-    up = lax.dot_general(own_rows, du[...], across, preferred_element_type=f32)
+    turned = (((1,), (1,)), ((), ()))
+    gate = lax.dot_general(own_rows, dg[...], turned, preferred_element_type=f32)
+    up = lax.dot_general(own_rows, du[...], turned, preferred_element_type=f32)
     mixed = (jax.nn.silu(gate) * up).astype(bf16)
     dens[...] = jnp.dot(mixed, dd[...], preferred_element_type=f32) * jax.nn.sigmoid(goff[...])
-    for q in range(zs):
+    for q in range(1, zs):
         for d in range(1, lanes):
-            hold_t[d, q].wait_recv()
+            hold[d, q].wait_recv()
             to_partner(d, q)
     for d in range(1, lanes):
         for q in range(zs):
@@ -487,16 +520,26 @@
     picked = lax.broadcasted_iota(jnp.int32, tail.shape, 1) % 64 == me_g
     scale = jnp.sum(jnp.where(picked, tail, 0.0), axis=-1, keepdims=True)
     pieces, wide = ys.shape[0], ys.shape[-1]
-    to_core, to_lane, to_z = [], [], []
+    to_core, to_lane, to_diag, to_last, to_z = [], [], [], [], []
 
     def pass_on(n):
         to_core[n].wait_recv()
         own = []
-        for d in range(1, lanes):
+        for q in range(1, zs):
+            i = n * (zs - 1) + q - 1
+            ys[n, 0, across, q] = (
+                ys[n, 0, across, q].astype(f32) + y_in[n, across, q].astype(f32)
+            ).astype(bf16)
+            own.append(
+                send(ys.at[n, 0, across, q], dg_in.at[n, q - 1], sg.at[i], rg.at[i], z_peer(-q))
+            )
+        to_diag.append(own)
+        own = []
+        for d in (1, 2):
             ys[n, 0, d] = (ys[n, 0, d].astype(f32) + y_in[n, d].astype(f32)).astype(bf16)
-            i = n * (lanes - 1) + d - 1
+            i = 2 * n + d - 1
             own.append(
-                send(ys.at[n, 0, d], z_in.at[n, d - 1], sb.at[i], rb.at[i], lane_peer(-d))
+                send(ys.at[n, 0, d], z_in.at[n, d - 1], sb.at[i], rb.at[i], lane_peer(d))
             )
         to_lane.append(own)
 
@@ -514,29 +557,37 @@
     pass_on(pieces - 1)
     for n in range(pieces):
         cols = slice(n * wide, (n + 1) * wide)
+        total = ys[n, 0, across, 0].astype(f32) + y_in[n, across, 0].astype(f32)
+        for q in range(1, zs):
+            to_diag[n][q - 1].wait_recv()
+            total = total + dg_in[n, q - 1].astype(f32)
+        d_out[n] = total.astype(bf16)
+        to_last.append(send(d_out.at[n], d_in.at[n], sd.at[n], rd.at[n], lane_peer(across)))
         total = ys[n, 0, 0].astype(f32) + y_in[n, 0].astype(f32)
-        for d in range(1, lanes):
+        for d in (1, 2):
             to_lane[n][d - 1].wait_recv()
             total = total + z_in[n, d - 1].astype(f32)
         v_out[n] = total.astype(bf16)
         own = []
-        for d in range(1, zs):
-            i = n * (zs - 1) + d - 1
+        for q in range(1, zs):
+            i = n * (zs - 1) + q - 1
             own.append(
-                send(v_out.at[n, d], v_in.at[n, d - 1], sv.at[i], rv.at[i], z_peer(-d))
+                send(v_out.at[n, q], v_in.at[n, q - 1], sv.at[i], rv.at[i], z_peer(-q))
             )
         to_z.append(own)
         hid_rows[:, cols] = hid_rows[:, cols] + total[0]
     for n in range(pieces):
         cols = slice(n * wide, (n + 1) * wide)
         result = hid_rows[:, cols]
+        to_last[n].wait_recv()
+        result = result + d_in[n].astype(f32)
         for d, copy in enumerate(to_z[n]):
             copy.wait_recv()
             result = result + v_in[n, d].astype(f32)
         out_ref[:, cols] = result.astype(bf16)
-    sent += list(hold_z.values()) + list(hold_t.values()) + list(hold_c.values())
-    sent += to_core
-    for own in to_lane + to_z:
+    sent += list(hold.values()) + list(hold_c.values())
+    sent += to_core + to_last
+    for own in to_lane + to_diag + to_z:
         sent += own
     for copy in sent:
         copy.wait_send()
@@ -588,8 +639,8 @@
     next_state, layer_rows = pl.pallas_call(
         functools.partial(fused_kernel, count, groups, lanes),
         out_shape=(
-            jax.ShapeDtypeStruct((heads, seqs, flat_width), f32),
-            jax.ShapeDtypeStruct((rows, width), bf16),
+            pltpu.VMEM((heads, seqs, flat_width), f32),
+            pltpu.VMEM((rows, width), bf16),
         ),
         in_specs=[anywhere] * (count + 9),
         out_specs=(vmem, vmem),
@@ -617,19 +668,23 @@
             pltpu.VMEM((2 * zs * rows, width), f32),
             pltpu.VMEM((pieces, 2, lanes, zs, rows, wide), bf16),
             pltpu.VMEM((pieces, lanes, zs, rows, wide), bf16),
-            pltpu.VMEM((pieces, lanes - 1, zs, rows, wide), bf16),
+            pltpu.VMEM((pieces, 2, zs, rows, wide), bf16),
             pltpu.VMEM((pieces, zs, rows, wide), bf16),
             pltpu.VMEM((pieces, zs - 1, rows, wide), bf16),
+            pltpu.VMEM((pieces, zs - 1, rows, wide), bf16),
+            pltpu.VMEM((pieces, rows, wide), bf16),
+            pltpu.VMEM((pieces, rows, wide), bf16),
             dma((count,)),
             dma((heads,)),
             dma((8,)),
             dma((lanes - 1,)), dma((lanes - 1,)),
-            dma((zs - 1,)), dma((zs - 1,)),
-            dma(((lanes - 1) * zs,)), dma(((lanes - 1) * zs,)),
+            dma((lanes * zs,)), dma((lanes * zs,)),
             dma((lanes * zs,)), dma((lanes * zs,)),
             dma((pieces,)), dma((pieces,)),
-            dma((pieces * (lanes - 1),)), dma((pieces * (lanes - 1),)),
+            dma((pieces * 2,)), dma((pieces * 2,)),
             dma((pieces * (zs - 1),)), dma((pieces * (zs - 1),)),
+            dma((pieces * (zs - 1),)), dma((pieces * (zs - 1),)),
+            dma((pieces,)), dma((pieces,)),
         ],
         compiler_params=pltpu.CompilerParams(
             collective_id=0, has_side_effects=True, vmem_limit_bytes=grant
@@ -649,8 +704,12 @@
         in_specs=[vmem, vmem],
         out_specs=(anywhere, anywhere),
         scratch_shapes=[dma, dma((heads,))],
+        compiler_params=pltpu.CompilerParams(vmem_limit_bytes=1 << 20),
         name="hand_over",
-    )(layer_rows, next_state)
+    )(
+        pltpu.with_memory_space_constraint(layer_rows, pltpu.VMEM),
+        pltpu.with_memory_space_constraint(next_state, pltpu.VMEM),
+    )
 
 
 def choose(tokens, recurrent_head_state, *rest):
@@ -658,7 +717,7 @@
     rows, heads = tokens.shape[0] // lanes, recurrent_head_state.shape[1]
     experts_here = rest[14].shape[0]
     fits = (
-        rows % 8 == 0 and heads % 2 == 0 and groups % 2 == 0 and groups > 2 and lanes > 1
+        rows % 8 == 0 and heads % 2 == 0 and groups % 2 == 0 and groups > 2 and lanes == 4
         and groups <= 64 and experts_here == 1
     )
     return (fused if fits else local)(tokens, recurrent_head_state, *rest)

time: 44.2 us -> 37.8 us (0.86)
  Pallas kernels: 43.4 us -> 37 us
    pallas_call x1, Pallas kernels: 40.4 us -> 35.6 us  [fused(): pl.pallas_call(functools.partial(fused_kernel, count, groups, lanes), out...]
    pallas_call x1, Pallas kernels: 2.98 us -> 1.37 us  [fused(): pl.pallas_call(hand_over_kernel, out_shape=(jax.ShapeDtypeStruct((rows, w...]
where the time goes in v2:
time: 37.8 us; the launch traced here: 37.6 us
  Pallas kernels  37 us (98%)
  between operations  0.65 us (2%)
    pallas_call x1, Pallas kernels, fused(): pl.pallas_call(functools.partial(fused_kernel, count, groups, lanes), out...  35.6 us
    pallas_call x1, Pallas kernels, fused(): pl.pallas_call(hand_over_kernel, out_shape=(jax.ShapeDtypeStruct((rows, w...  1.37 us

profile of v2, /device:TPU:0, one launch (start us, length us, event | category | flops | bytes accessed | tf_op | source)
XLA Modules:
  0.0 37.6 jit_solution(17203590408324981035)
XLA Ops:
  0.6 35.6 %layer.1 = (f32[4,32,4096]{2,1,0:T(8,128)S(1)}, bf16[8,2048]{1,0:T(8,128)(2,1)S(1)}) custom-call(bf16[32,2048]{1,0:T(8,128)(2,1)} %refs_0_.1, f32[1,2048]{1,0:T(1,128)} %bitcast.14, f32[1,256]{1,0:T(1,128)} %bitcast.18, f32[1,256]{1,0:T(1,128)} %bitcast.19, f32[1,256]{1,0:T(1,128)} %bitcast.20, f32[1,256]{1,0:T(1,128)} %bitcast.21, f32[1,256]{1,0:T(1,128)} %bitcast.22, ...), custom_call_target="tpu_custom_call" | custom-call | tf_op jit(solution)/shard_map/layer/pallas_call | solution.py:639
  36.3 1.4 %hand_over.1 = (bf16[8,2048]{1,0:T(8,128)(2,1)}, f32[32,4,4096]{2,1,0:T(4,128)}) custom-call(bf16[8,2048]{1,0:T(8,128)(2,1)S(1)} %get-tuple-element.4.rows_ref, f32[4,32,4096]{2,1,0:T(8,128)S(1)} %get-tuple-element.5.state_ref), custom_call_target="tpu_custom_call" | custom-call | tf_op jit(solution)/shard_map/hand_over/pallas_call | solution.py:698

commit v3 on v2

--- a/solution.py
+++ b/solution.py
@@ -234,8 +234,11 @@
     def lane_peer(d):
         return (me_g, lane_at(d))
 
-    def z_peer(d):
-        return (lax.rem(me_z + d + zs, zs) * 2 + core, me_l)
+    def far_lane(d):
+        return (partner[0], lane_at(d))
+
+    def far_z(d):
+        return (lax.rem(me_z + d + zs, zs) * 2 + 1 - core, me_l)
 
     def send(src, dst, ssem, rsem, peer):
         copy = pltpu.make_async_remote_copy(
@@ -244,6 +247,12 @@
         )
         copy.start()
         return copy
+
+    def whole(ref, sem):
+        return pltpu.make_async_remote_copy(
+            src_ref=ref, dst_ref=ref, send_sem=sem, recv_sem=sem, device_id=partner,
+            device_id_type=pl.DeviceIdType.MESH,
+        )
 
     seqs, width = tokens_ref.shape
     heads = state_ref.shape[1]
@@ -262,7 +271,8 @@
     for arg in args[-2:]:
         arg.start()
     barrier = pltpu.get_barrier_semaphore()
-    peers = [lane_peer(d) for d in range(1, lanes)] + [z_peer(d) for d in range(1, zs)] + [partner]
+    peers = [lane_peer(d) for d in range(1, lanes)] + [far_lane(d) for d in range(1, lanes)]
+    peers += [far_z(d) for d in range(1, zs)] + [partner]
     for peer in peers:
         pl.semaphore_signal(barrier, inc=1, device_id=peer, device_id_type=pl.DeviceIdType.MESH)
 
@@ -383,15 +393,9 @@
         base = jnp.where(me_l == i, mine + toks[i * rows : (i + 1) * rows], base)
     hid_rows[...] = base
     pl.semaphore_wait(barrier, len(peers))
-    sent = []
-    firsts = []
     across = lanes - 1
     for d in (across, 1, 2):
-        firsts.append(
-            send(
-                part_ref.at[lane_at(d)], p_in.at[d - 1], s1.at[d - 1], r1.at[d - 1], lane_peer(d)
-            )
-        )
+        send(part_ref.at[lane_at(d)], p_in.at[d - 1], s1, r1, lane_peer(d))
     pulls = [
         pltpu.make_async_copy(src, dst, w_sem.at[i])
         for i, (src, dst) in enumerate(
@@ -435,11 +439,9 @@
                     + came[:, i : i + pair] * ins[h]
                 )
     hidden = hid_rows[...]
-    for copy in firsts:
-        copy.wait_recv()
+    whole(p_in, r1).wait_recv()
     for d in range(1, lanes):
         hidden = hidden + p_in[d - 1].astype(f32)
-    sent += firsts
     hid_rows[...] = hidden
     for pull in pulls[:2]:
         pull.wait()
@@ -448,33 +450,31 @@
     hold = {}
 
     def pass_block(d, q, to_d, to_q, peer):
-        i = to_d * zs + to_q
-        hold[to_d, to_q] = send(xs.at[0, d, q], xs.at[0, to_d, to_q], st.at[i], rt.at[i], peer)
-
-    hold_c = {}
+        hold[to_d, to_q] = send(
+            xs.at[0, d, q], xs.at[0, to_d, to_q], st.at[0 if (d, q) == (0, 0) else 1],
+            rt.at[to_d * zs + to_q], peer,
+        )
 
     def to_partner(d, q):
-        i = d * zs + q
-        hold_c[d, q] = send(xs.at[0, d, q], xs.at[1, d, q], sc.at[i], rc.at[i], partner)
-
-    pass_block(0, 0, across, 0, lane_peer(across))
+        send(xs.at[0, d, q], xs.at[1, d, q], sc, rc.at[0 if d == 0 else 1], partner)
+
+    pass_block(0, 0, across, 0, far_lane(across))
     for q in range(1, zs):
-        pass_block(0, 0, 0, q, z_peer(q))
+        pass_block(0, 0, 0, q, far_z(q))
     for d in (1, 2):
-        pass_block(0, 0, d, 0, lane_peer(d))
+        pass_block(0, 0, d, 0, far_lane(d))
     to_partner(0, 0)
 
     def spread_row(q):
         hold[0, q].wait_recv()
         for d in (1, 2):
-            pass_block(0, q, d, q, lane_peer(d))
+            pass_block(0, q, d, q, far_lane(d))
         to_partner(0, q)
 
-    spread_row(1)
     hold[across, 0].wait_recv()
     for q in range(1, zs):
-        pass_block(across, 0, across, q, z_peer(q))
-    for q in range(2, zs):
+        pass_block(across, 0, across, q, far_z(q))
+    for q in range(zs - 1, 0, -1):
         spread_row(q)
     to_partner(across, 0)
     for d in (1, 2):
@@ -485,8 +485,7 @@
     def gathered(d):
         return xs[:, d].astype(f32).reshape(block, width + 128)
 
-    for q in range(zs):
-        hold_c[0, q].wait_recv()
+    whole(xs.at[1, 0], rc.at[0]).wait_recv()
     mine = gathered(0)
     flat[0:block] = mine.astype(bf16)
     own_rows = mine[:, :width].astype(bf16)
@@ -497,13 +496,12 @@
     up = lax.dot_general(own_rows, du[...], turned, preferred_element_type=f32)
     mixed = (jax.nn.silu(gate) * up).astype(bf16)
     dens[...] = jnp.dot(mixed, dd[...], preferred_element_type=f32) * jax.nn.sigmoid(goff[...])
-    for q in range(1, zs):
+    for q in range(zs - 1, 0, -1):
         for d in range(1, lanes):
             hold[d, q].wait_recv()
             to_partner(d, q)
+    whole(xs.at[1, 1:], rc.at[1]).wait_recv()
     for d in range(1, lanes):
-        for q in range(zs):
-            hold_c[d, q].wait_recv()
         flat[d * block : (d + 1) * block] = gathered(d).astype(bf16)
     for pull in pulls[5:]:
         pull.wait()
@@ -520,28 +518,17 @@
     picked = lax.broadcasted_iota(jnp.int32, tail.shape, 1) % 64 == me_g
     scale = jnp.sum(jnp.where(picked, tail, 0.0), axis=-1, keepdims=True)
     pieces, wide = ys.shape[0], ys.shape[-1]
-    to_core, to_lane, to_diag, to_last, to_z = [], [], [], [], []
 
     def pass_on(n):
-        to_core[n].wait_recv()
-        own = []
+        whole(y_in.at[n], ra.at[n]).wait_recv()
         for q in range(1, zs):
-            i = n * (zs - 1) + q - 1
             ys[n, 0, across, q] = (
                 ys[n, 0, across, q].astype(f32) + y_in[n, across, q].astype(f32)
             ).astype(bf16)
-            own.append(
-                send(ys.at[n, 0, across, q], dg_in.at[n, q - 1], sg.at[i], rg.at[i], z_peer(-q))
-            )
-        to_diag.append(own)
-        own = []
+            send(ys.at[n, 0, across, q], dg_in.at[n, q - 1], sg, rg.at[n], far_z(-q))
         for d in (1, 2):
             ys[n, 0, d] = (ys[n, 0, d].astype(f32) + y_in[n, d].astype(f32)).astype(bf16)
-            i = 2 * n + d - 1
-            own.append(
-                send(ys.at[n, 0, d], z_in.at[n, d - 1], sb.at[i], rb.at[i], lane_peer(d))
-            )
-        to_lane.append(own)
+            send(ys.at[n, 0, d], z_in.at[n, d - 1], sb, rb.at[n], far_lane(d))
 
     for n in range(pieces):
         cols = slice(n * wide, (n + 1) * wide)
@@ -551,46 +538,44 @@
             if d == 0:
                 piece = piece + dens[:, cols]
             ys[n, :, d] = piece.reshape(2, zs, rows, wide).astype(bf16)
-        to_core.append(send(ys.at[n, 1], y_in.at[n], sa.at[n], ra.at[n], partner))
+        send(ys.at[n, 1], y_in.at[n], sa, ra.at[n], partner)
         if n > 0:
             pass_on(n - 1)
     pass_on(pieces - 1)
     for n in range(pieces):
         cols = slice(n * wide, (n + 1) * wide)
         total = ys[n, 0, across, 0].astype(f32) + y_in[n, across, 0].astype(f32)
+        whole(dg_in.at[n], rg.at[n]).wait_recv()
         for q in range(1, zs):
-            to_diag[n][q - 1].wait_recv()
             total = total + dg_in[n, q - 1].astype(f32)
         d_out[n] = total.astype(bf16)
-        to_last.append(send(d_out.at[n], d_in.at[n], sd.at[n], rd.at[n], lane_peer(across)))
+        send(d_out.at[n], d_in.at[n], sd, rd.at[n], far_lane(across))
         total = ys[n, 0, 0].astype(f32) + y_in[n, 0].astype(f32)
+        whole(z_in.at[n], rb.at[n]).wait_recv()
         for d in (1, 2):
-            to_lane[n][d - 1].wait_recv()
             total = total + z_in[n, d - 1].astype(f32)
         v_out[n] = total.astype(bf16)
-        own = []
         for q in range(1, zs):
-            i = n * (zs - 1) + q - 1
-            own.append(
-                send(v_out.at[n, q], v_in.at[n, q - 1], sv.at[i], rv.at[i], z_peer(-q))
-            )
-        to_z.append(own)
+            send(v_out.at[n, q], v_in.at[n, q - 1], sv, rv.at[n], far_z(-q))
         hid_rows[:, cols] = hid_rows[:, cols] + total[0]
+    whole(p_in, s1).wait_send()
+    whole(xs.at[:, 1:, 0], st.at[0]).wait_send()
+    whole(xs.at[0, 1:, 1:], st.at[1]).wait_send()
+    whole(xs.at[1], sc).wait_send()
+    whole(y_in, sa).wait_send()
+    whole(dg_in, sg).wait_send()
+    whole(z_in, sb).wait_send()
     for n in range(pieces):
         cols = slice(n * wide, (n + 1) * wide)
         result = hid_rows[:, cols]
-        to_last[n].wait_recv()
+        whole(d_in.at[n], rd.at[n]).wait_recv()
+        whole(v_in.at[n], rv.at[n]).wait_recv()
         result = result + d_in[n].astype(f32)
-        for d, copy in enumerate(to_z[n]):
-            copy.wait_recv()
-            result = result + v_in[n, d].astype(f32)
+        for q in range(1, zs):
+            result = result + v_in[n, q - 1].astype(f32)
         out_ref[:, cols] = result.astype(bf16)
-    sent += list(hold.values()) + list(hold_c.values())
-    sent += to_core + to_last
-    for own in to_lane + to_diag + to_z:
-        sent += own
-    for copy in sent:
-        copy.wait_send()
+    whole(v_in, sv).wait_send()
+    whole(d_in, sd).wait_send()
 
 
 def hand_over_kernel(rows_ref, state_ref, out_ref, next_ref, row_sem, state_sem):
@@ -677,14 +662,9 @@
             dma((count,)),
             dma((heads,)),
             dma((8,)),
-            dma((lanes - 1,)), dma((lanes - 1,)),
-            dma((lanes * zs,)), dma((lanes * zs,)),
-            dma((lanes * zs,)), dma((lanes * zs,)),
-            dma((pieces,)), dma((pieces,)),
-            dma((pieces * 2,)), dma((pieces * 2,)),
-            dma((pieces * (zs - 1),)), dma((pieces * (zs - 1),)),
-            dma((pieces * (zs - 1),)), dma((pieces * (zs - 1),)),
-            dma((pieces,)), dma((pieces,)),
+            dma, dma, dma((2,)), dma((lanes * zs,)), dma, dma((2,)),
+            dma, dma((pieces,)), dma, dma((pieces,)), dma, dma((pieces,)),
+            dma, dma((pieces,)), dma, dma((pieces,)),
         ],
         compiler_params=pltpu.CompilerParams(
             collective_id=0, has_side_effects=True, vmem_limit_bytes=grant

time: 37.8 us -> 35.4 us (0.937)
  Pallas kernels: 37 us -> 34.6 us
    pallas_call x1, Pallas kernels: 35.6 us -> 33.2 us  [fused(): pl.pallas_call(functools.partial(fused_kernel, count, groups, lanes), out...]
where the time goes in v3:
time: 35.4 us; the launch traced here: 35.2 us
  Pallas kernels  34.6 us (98%)
  between operations  0.65 us (2%)
    pallas_call x1, Pallas kernels, fused(): pl.pallas_call(functools.partial(fused_kernel, count, groups, lanes), out...  33.2 us
    pallas_call x1, Pallas kernels, fused(): pl.pallas_call(hand_over_kernel, out_shape=(jax.ShapeDtypeStruct((rows, w...  1.37 us

profile of v3, /device:TPU:0, one launch (start us, length us, event | category | flops | bytes accessed | tf_op | source)
XLA Modules:
  0.0 35.2 jit_solution(13467849135633789115)
XLA Ops:
  0.6 33.2 %layer.1 = (f32[4,32,4096]{2,1,0:T(8,128)S(1)}, bf16[8,2048]{1,0:T(8,128)(2,1)S(1)}) custom-call(bf16[32,2048]{1,0:T(8,128)(2,1)} %refs_0_.1, f32[1,2048]{1,0:T(1,128)} %bitcast.14, f32[1,256]{1,0:T(1,128)} %bitcast.18, f32[1,256]{1,0:T(1,128)} %bitcast.19, f32[1,256]{1,0:T(1,128)} %bitcast.20, f32[1,256]{1,0:T(1,128)} %bitcast.21, f32[1,256]{1,0:T(1,128)} %bitcast.22, ...), custom_call_target="tpu_custom_call" | custom-call | tf_op jit(solution)/shard_map/layer/pallas_call | solution.py:624
  33.8 1.4 %hand_over.1 = (bf16[8,2048]{1,0:T(8,128)(2,1)}, f32[32,4,4096]{2,1,0:T(4,128)}) custom-call(bf16[8,2048]{1,0:T(8,128)(2,1)S(1)} %get-tuple-element.4.rows_ref, f32[4,32,4096]{2,1,0:T(8,128)S(1)} %get-tuple-element.5.state_ref), custom_call_target="tpu_custom_call" | custom-call | tf_op jit(solution)/shard_map/hand_over/pallas_call | solution.py:678

commit v4 on v3

--- a/solution.py
+++ b/solution.py
@@ -352,6 +352,16 @@
         load.wait()
     args[12].wait()
     values = jnp.dot(normed, wv_ref[...], preferred_element_type=f32)
+    pulls = [
+        pltpu.make_async_copy(src, dst, w_sem.at[i])
+        for i, (src, dst) in enumerate(
+            [(gain_hbm, gain), (goff_hbm, goff), (dg_hbm, dg), (du_hbm, du), (dd_hbm, dd),
+             (eg_hbm.at[0], eg), (eu_hbm.at[0], eu), (ed_hbm.at[0], ed)]
+        )
+    ]
+    for pull in pulls:
+        pull.start()
+
     (key_squares,) = group_sums(keys * keys)
     rate = jax.nn.sigmoid(coff_ref[...] + cfac_ref[...] * keys)
     unit = keys * lax.rsqrt(key_squares * (1.0 / HEAD_WIDTH) + 1e-06) * HEAD_WIDTH ** (-0.5)
@@ -396,16 +406,6 @@
     across = lanes - 1
     for d in (across, 1, 2):
         send(part_ref.at[lane_at(d)], p_in.at[d - 1], s1, r1, lane_peer(d))
-    pulls = [
-        pltpu.make_async_copy(src, dst, w_sem.at[i])
-        for i, (src, dst) in enumerate(
-            [(gain_hbm, gain), (goff_hbm, goff), (dg_hbm, dg), (du_hbm, du), (dd_hbm, dd),
-             (eg_hbm.at[0], eg), (eu_hbm.at[0], eu), (ed_hbm.at[0], ed)]
-        )
-    ]
-    for pull in pulls:
-        pull.start()
-
     offset = (
         lax.broadcasted_iota(jnp.int32, (pair, tile), 0) % HEAD_WIDTH
         - lax.broadcasted_iota(jnp.int32, (pair, tile), 1) // HEAD_WIDTH
@@ -517,47 +517,52 @@
     tail = flat[:, width:].astype(f32)
     picked = lax.broadcasted_iota(jnp.int32, tail.shape, 1) % 64 == me_g
     scale = jnp.sum(jnp.where(picked, tail, 0.0), axis=-1, keepdims=True)
-    pieces, wide = ys.shape[0], ys.shape[-1]
+    pieces = 4
+    edges = [n * (width // pieces) for n in range(pieces + 1)]
+    spans = [slice(low_edge, high_edge) for low_edge, high_edge in zip(edges, edges[1:])]
 
     def pass_on(n):
-        whole(y_in.at[n], ra.at[n]).wait_recv()
+        cols = spans[n]
+        whole(y_in.at[:, :, :, cols], ra.at[n]).wait_recv()
         for q in range(1, zs):
-            ys[n, 0, across, q] = (
-                ys[n, 0, across, q].astype(f32) + y_in[n, across, q].astype(f32)
+            ys[0, across, q, :, cols] = (
+                ys[0, across, q, :, cols].astype(f32) + y_in[across, q, :, cols].astype(f32)
             ).astype(bf16)
-            send(ys.at[n, 0, across, q], dg_in.at[n, q - 1], sg, rg.at[n], far_z(-q))
+            send(ys.at[0, across, q, :, cols], dg_in.at[q - 1, :, cols], sg, rg.at[n], far_z(-q))
         for d in (1, 2):
-            ys[n, 0, d] = (ys[n, 0, d].astype(f32) + y_in[n, d].astype(f32)).astype(bf16)
-            send(ys.at[n, 0, d], z_in.at[n, d - 1], sb, rb.at[n], far_lane(d))
+            ys[0, d, :, :, cols] = (ys[0, d, :, :, cols].astype(f32) + y_in[d, :, :, cols].astype(f32)).astype(bf16)
+            send(ys.at[0, d, :, :, cols], z_in.at[d - 1, :, :, cols], sb, rb.at[n], far_lane(d))
 
     for n in range(pieces):
-        cols = slice(n * wide, (n + 1) * wide)
+        cols = spans[n]
+        wide = cols.stop - cols.start
         made = jnp.dot(hid[...], ed[:, cols], preferred_element_type=f32) * scale
         for d in range(lanes):
             piece = made[d * block : (d + 1) * block]
             if d == 0:
                 piece = piece + dens[:, cols]
-            ys[n, :, d] = piece.reshape(2, zs, rows, wide).astype(bf16)
-        send(ys.at[n, 1], y_in.at[n], sa, ra.at[n], partner)
+            ys[:, d, :, :, cols] = piece.reshape(2, zs, rows, wide).astype(bf16)
+        send(ys.at[1, :, :, :, cols], y_in.at[:, :, :, cols], sa, ra.at[n], partner)
         if n > 0:
             pass_on(n - 1)
     pass_on(pieces - 1)
     for n in range(pieces):
-        cols = slice(n * wide, (n + 1) * wide)
-        total = ys[n, 0, across, 0].astype(f32) + y_in[n, across, 0].astype(f32)
-        whole(dg_in.at[n], rg.at[n]).wait_recv()
+        cols = spans[n]
+        wide = cols.stop - cols.start
+        total = ys[0, 0, :, :, cols].astype(f32) + y_in[0, :, :, cols].astype(f32)
+        whole(z_in.at[:, :, :, cols], rb.at[n]).wait_recv()
+        for d in (1, 2):
+            total = total + z_in[d - 1, :, :, cols].astype(f32)
+        v_out[:, :, cols] = total.astype(bf16)
         for q in range(1, zs):
-            total = total + dg_in[n, q - 1].astype(f32)
-        d_out[n] = total.astype(bf16)
-        send(d_out.at[n], d_in.at[n], sd, rd.at[n], far_lane(across))
-        total = ys[n, 0, 0].astype(f32) + y_in[n, 0].astype(f32)
-        whole(z_in.at[n], rb.at[n]).wait_recv()
-        for d in (1, 2):
-            total = total + z_in[n, d - 1].astype(f32)
-        v_out[n] = total.astype(bf16)
+            send(v_out.at[q, :, cols], v_in.at[q - 1, :, cols], sv, rv.at[n], far_z(-q))
+        hid_rows[:, cols] = hid_rows[:, cols] + total[0]
+        total = ys[0, across, 0, :, cols].astype(f32) + y_in[across, 0, :, cols].astype(f32)
+        whole(dg_in.at[:, :, cols], rg.at[n]).wait_recv()
         for q in range(1, zs):
-            send(v_out.at[n, q], v_in.at[n, q - 1], sv, rv.at[n], far_z(-q))
-        hid_rows[:, cols] = hid_rows[:, cols] + total[0]
+            total = total + dg_in[q - 1, :, cols].astype(f32)
+        d_out[:, cols] = total.astype(bf16)
+        send(d_out.at[:, cols], d_in.at[:, cols], sd, rd.at[n], far_lane(across))
     whole(p_in, s1).wait_send()
     whole(xs.at[:, 1:, 0], st.at[0]).wait_send()
     whole(xs.at[0, 1:, 1:], st.at[1]).wait_send()
@@ -566,13 +571,14 @@
     whole(dg_in, sg).wait_send()
     whole(z_in, sb).wait_send()
     for n in range(pieces):
-        cols = slice(n * wide, (n + 1) * wide)
+        cols = spans[n]
+        wide = cols.stop - cols.start
         result = hid_rows[:, cols]
-        whole(d_in.at[n], rd.at[n]).wait_recv()
-        whole(v_in.at[n], rv.at[n]).wait_recv()
-        result = result + d_in[n].astype(f32)
+        whole(d_in.at[:, cols], rd.at[n]).wait_recv()
+        whole(v_in.at[:, :, cols], rv.at[n]).wait_recv()
+        result = result + d_in[:, cols].astype(f32)
         for q in range(1, zs):
-            result = result + v_in[n, q - 1].astype(f32)
+            result = result + v_in[q - 1, :, cols].astype(f32)
         out_ref[:, cols] = result.astype(bf16)
     whole(v_in, sv).wait_send()
     whole(d_in, sd).wait_send()
@@ -618,7 +624,6 @@
     count = len(operands)
     hidden_units = expert_gate_weight.shape[2]
     pieces = 4
-    wide = width // pieces
     total = groups * seqs
     pair = 2 * HEAD_WIDTH
     next_state, layer_rows = pl.pallas_call(
@@ -651,14 +656,14 @@
             pltpu.VMEM((total, width + 128), bf16),
             pltpu.VMEM((total, hidden_units), bf16),
             pltpu.VMEM((2 * zs * rows, width), f32),
-            pltpu.VMEM((pieces, 2, lanes, zs, rows, wide), bf16),
-            pltpu.VMEM((pieces, lanes, zs, rows, wide), bf16),
-            pltpu.VMEM((pieces, 2, zs, rows, wide), bf16),
-            pltpu.VMEM((pieces, zs, rows, wide), bf16),
-            pltpu.VMEM((pieces, zs - 1, rows, wide), bf16),
-            pltpu.VMEM((pieces, zs - 1, rows, wide), bf16),
-            pltpu.VMEM((pieces, rows, wide), bf16),
-            pltpu.VMEM((pieces, rows, wide), bf16),
+            pltpu.VMEM((2, lanes, zs, rows, width), bf16),
+            pltpu.VMEM((lanes, zs, rows, width), bf16),
+            pltpu.VMEM((2, zs, rows, width), bf16),
+            pltpu.VMEM((zs, rows, width), bf16),
+            pltpu.VMEM((zs - 1, rows, width), bf16),
+            pltpu.VMEM((zs - 1, rows, width), bf16),
+            pltpu.VMEM((rows, width), bf16),
+            pltpu.VMEM((rows, width), bf16),
             dma((count,)),
             dma((heads,)),
             dma((8,)),

time: 35.4 us -> 35 us (0.989)
  Pallas kernels: 34.6 us -> 34.2 us
where the time goes in v4:
time: 35 us; the launch traced here: 34.9 us
  Pallas kernels  34.2 us (98%)
  between operations  0.65 us (2%)
    pallas_call x1, Pallas kernels, fused(): pl.pallas_call(functools.partial(fused_kernel, count, groups, lanes), out...  32.8 us
    pallas_call x1, Pallas kernels, fused(): pl.pallas_call(hand_over_kernel, out_shape=(jax.ShapeDtypeStruct((rows, w...  1.37 us

profile of v4, /device:TPU:0, one launch (start us, length us, event | category | flops | bytes accessed | tf_op | source)
XLA Modules:
  0.0 34.9 jit_solution(6709303013035909790)
XLA Ops:
  0.6 32.8 %layer.1 = (f32[4,32,4096]{2,1,0:T(8,128)S(1)}, bf16[8,2048]{1,0:T(8,128)(2,1)S(1)}) custom-call(bf16[32,2048]{1,0:T(8,128)(2,1)} %refs_0_.1, f32[1,2048]{1,0:T(1,128)} %bitcast.14, f32[1,256]{1,0:T(1,128)} %bitcast.18, f32[1,256]{1,0:T(1,128)} %bitcast.19, f32[1,256]{1,0:T(1,128)} %bitcast.20, f32[1,256]{1,0:T(1,128)} %bitcast.21, f32[1,256]{1,0:T(1,128)} %bitcast.22, ...), custom_call_target="tpu_custom_call" | custom-call | tf_op jit(solution)/shard_map/layer/pallas_call | solution.py:629
  33.5 1.4 %hand_over.1 = (bf16[8,2048]{1,0:T(8,128)(2,1)}, f32[32,4,4096]{2,1,0:T(4,128)}) custom-call(bf16[8,2048]{1,0:T(8,128)(2,1)S(1)} %get-tuple-element.4.rows_ref, f32[4,32,4096]{2,1,0:T(8,128)S(1)} %get-tuple-element.5.state_ref), custom_call_target="tpu_custom_call" | custom-call | tf_op jit(solution)/shard_map/hand_over/pallas_call | solution.py:683
